TPU v7x, 32 devices: a whole 2x2x4 slice. The times are simulated.
32 devices in a mesh: ep: 8 (over z, x), tp: 4 (over y, core).
Axes of the slice: x: 2, y: 2, z: 4, core: 2. Of those that a mesh axis runs over, the one named last changes fastest.
Arguments:
- tokens: bfloat16 [1024, 2048], P('ep'), may hold values from -6 to 6
- cotangent: bfloat16 [1024, 2048], P('ep'), may hold values from -1.5 to 1.5
- routes: int32 [1024, 2], P('ep'), may hold values from 0 to 3, all different within a row; in each aligned block of 128 rows (0 to 127, 128 to 255, ...) at most 96 rows name the same one
- router: bfloat16 [2048, 4], replicated, may hold values from -0.125 to 0.125
- w_gate: bfloat16 [8, 2048, 2048], P('ep', None, 'tp'), may hold values from -0.125 to 0.125
- w_up: bfloat16 [8, 2048, 2048], P('ep', None, 'tp'), may hold values from -0.125 to 0.125
- w_down: bfloat16 [8, 2048, 2048], P('ep', 'tp'), may hold values from -0.09375 to 0.09375
Outputs:
- token_grad: bfloat16 [1024, 2048], P('ep', 'tp')
- gate_grad: float32 [1024, 2], P('ep')
- grad_gate: bfloat16 [8, 2048, 2048], P('ep', None, 'tp')
- grad_up: bfloat16 [8, 2048, 2048], P('ep', None, 'tp')
- grad_down: bfloat16 [8, 2048, 2048], P('ep', 'tp')
- router_grad: float32 [2048, 4], P(('ep', 'tp'))
Inputs may be any that keep to these rules, and one draw needn't show every extreme that they name: `routes`: each row names 2 different experts. In the rows of one index of ep (aligned blocks of 128 rows) no expert is named by more than 96 rows, a bound that some block reaches.
All inputs are finite; a program needn't handle non-finite values.
Results may differ from a plain program's by a relative error of at most 0.018.
Values may be sent and summed in bfloat16 or wider, within the bound.
No kernel may reach another device: no remote copies, remote signals or barrier semaphores. Data moves between devices by JAX's collectives and lax.ppermute only.
A program may use at most 64 MiB of HBM per device.

v0:
```python
import jax
import jax.numpy as jnp
from jax import lax
from jax.sharding import PartitionSpec as P

BLOCKS = 2


def build_slots(block_routes, experts, capacity):
    flat_routes = block_routes.reshape(-1)
    labels = jnp.arange(experts, dtype=jnp.int32)
    hit_mask = (flat_routes[None, :] == labels[:, None]).astype(jnp.int32)
    rank_in = jnp.cumsum(hit_mask, axis=1, dtype=jnp.int32) - 1
    slot_ids = jnp.arange(capacity, dtype=jnp.int32)
    assigned = (hit_mask[:, None, :] == 1) & (rank_in[:, None, :] == slot_ids[None, :, None])
    return assigned.astype(jnp.float32)


def gate_pair(tokens, routes, router, experts):
    logits = jnp.dot(tokens, router, preferred_element_type=jnp.float32)
    labels = jnp.arange(experts, dtype=jnp.int32)
    picked = (routes[:, :, None] == labels[None, None, :]).astype(jnp.float32)
    chosen = jnp.sum(picked * logits[:, None, :], axis=2)
    margin = chosen[:, 0] - chosen[:, 1]
    weights = jnp.stack([jax.nn.sigmoid(margin), jax.nn.sigmoid(-margin)], axis=1)
    return (picked, weights)


def logit_grads(picked, weights, gate_grad):
    lead_grad = weights[:, 0] * weights[:, 1] * (gate_grad[:, 0] - gate_grad[:, 1])
    pair_grad = jnp.stack([lead_grad, -lead_grad], axis=1)
    return jnp.sum(picked * pair_grad[:, :, None], axis=1)


def expert_grads(rows_in, cot_in, gate_in, gate_weight, up_weight, down_weight):
    pre_gate = jnp.dot(rows_in, gate_weight, preferred_element_type=jnp.float32)
    pre_up = jnp.dot(rows_in, up_weight, preferred_element_type=jnp.float32)
    back_grad = lax.dot_general(
        cot_in, down_weight, (((1,), (1,)), ((), ())), preferred_element_type=jnp.float32
    )
    sig_gate = jax.nn.sigmoid(pre_gate)
    active = pre_gate * sig_gate
    hidden = (active * pre_up).astype(jnp.bfloat16)
    gate_terms = jnp.sum(hidden.astype(jnp.float32) * back_grad, axis=1)
    gate_col = gate_in.astype(jnp.float32)[:, None]
    scaled_back = gate_col * back_grad
    d_gate = (scaled_back * pre_up * sig_gate * (1.0 + pre_gate * (1.0 - sig_gate))).astype(
        jnp.bfloat16
    )
    d_up = (scaled_back * active).astype(jnp.bfloat16)
    scaled_cot = (gate_col * cot_in.astype(jnp.float32)).astype(jnp.bfloat16)
    contract_rows = (((0,), (0,)), ((), ()))
    grad_gate = lax.dot_general(
        rows_in, d_gate, contract_rows, preferred_element_type=jnp.float32
    ).astype(jnp.bfloat16)
    grad_up = lax.dot_general(
        rows_in, d_up, contract_rows, preferred_element_type=jnp.float32
    ).astype(jnp.bfloat16)
    grad_down = lax.dot_general(
        hidden, scaled_cot, contract_rows, preferred_element_type=jnp.float32
    ).astype(jnp.bfloat16)
    return (d_gate, d_up, gate_terms, grad_gate, grad_up, grad_down)


def spread_slabs(packed, experts, slab_count):
    widened = jnp.broadcast_to(packed[:, None], (experts, BLOCKS) + packed.shape[1:])
    return widened.reshape((slab_count,) + packed.shape[1:])


def shards(tokens, cotangent, routes, router, w_gate, w_up, w_down):
    highest = lax.Precision.HIGHEST
    ep_count = lax.axis_size("ep")
    tp_count = lax.axis_size("tp")
    experts = ep_count // BLOCKS
    tok_rows, width = tokens.shape
    top_count = routes.shape[1]
    capacity = 3 * tok_rows * top_count // (2 * experts)
    col_width = width // tp_count
    tp_index = lax.axis_index("tp")
    picked, weights = gate_pair(tokens, routes, router, experts)
    assigned = build_slots(routes, experts, capacity)
    per_token = jnp.sum(assigned.reshape(experts, capacity, tok_rows, top_count), axis=3)
    token_map = per_token.astype(jnp.bfloat16)
    gate_send = weights.astype(jnp.bfloat16)
    gate_slots = jnp.einsum(
        "ecj,j->ec", assigned, gate_send.astype(jnp.float32).reshape(-1), precision=highest
    ).astype(jnp.bfloat16)
    gate_out = spread_slabs(gate_slots, experts, ep_count)

    def pack_rows(source):
        packed = jnp.einsum(
            "ect,td->ecd", token_map, source, preferred_element_type=jnp.float32
        ).astype(jnp.bfloat16)
        return spread_slabs(packed, experts, ep_count)

    tok_part = lax.dynamic_slice_in_dim(tokens, tp_index * col_width, col_width, 1)
    cot_part = lax.dynamic_slice_in_dim(cotangent, tp_index * col_width, col_width, 1)
    recv_part, recv_cot_part, recv_gate = (
        lax.all_to_all(pack_rows(tok_part), "ep", split_axis=0, concat_axis=0, tiled=True),
        lax.all_to_all(pack_rows(cot_part), "ep", split_axis=0, concat_axis=0, tiled=True),
        lax.all_to_all(gate_out, "ep", split_axis=0, concat_axis=0, tiled=True),
    )
    recv_rows, recv_cot = (
        lax.all_gather(recv_part, "tp", axis=2, tiled=True),
        lax.all_gather(recv_cot_part, "tp", axis=2, tiled=True),
    )
    rows_in = recv_rows.reshape(-1, width)
    cot_in = recv_cot.reshape(-1, width)
    gate_in = recv_gate.reshape(-1)
    d_gate, d_up, gate_terms, grad_gate, grad_up, grad_down = expert_grads(
        rows_in, cot_in, gate_in, w_gate[0], w_up[0], w_down[0]
    )
    contract_hidden = (((1,), (1,)), ((), ()))
    partial_dx = lax.dot_general(
        d_gate, w_gate[0], contract_hidden, preferred_element_type=jnp.float32
    )
    partial_dx = partial_dx + lax.dot_general(
        d_up, w_up[0], contract_hidden, preferred_element_type=jnp.float32
    )
    summed_dx = lax.psum_scatter(
        partial_dx.reshape(ep_count, capacity, width).astype(jnp.bfloat16),
        "tp",
        scatter_dimension=2,
        tiled=True,
    ).astype(jnp.float32)
    gate_sums = lax.psum(gate_terms.reshape(ep_count, capacity), "tp")
    back_dx, back_gate = (
        lax.all_to_all(
            summed_dx.astype(jnp.bfloat16), "ep", split_axis=0, concat_axis=0, tiled=True
        ).astype(summed_dx.dtype),
        lax.all_to_all(
            gate_sums.astype(jnp.bfloat16), "ep", split_axis=0, concat_axis=0, tiled=True
        ).astype(gate_sums.dtype),
    )
    slab_dx = jnp.sum(back_dx.reshape(experts, BLOCKS, capacity, col_width), axis=1)
    routed_dx = jnp.einsum("ect,ecd->td", per_token, slab_dx, precision=highest)
    slab_gate = jnp.sum(back_gate.reshape(experts, BLOCKS, capacity), axis=1)
    gate_grad = jnp.einsum("ecj,ec->j", assigned, slab_gate, precision=highest).reshape(
        tok_rows, top_count
    )
    logit_grad = logit_grads(picked, weights, gate_grad)
    router_cols = lax.dynamic_slice_in_dim(router, tp_index * col_width, col_width, 0).astype(
        jnp.float32
    )
    token_grad = (routed_dx + jnp.dot(logit_grad, router_cols.T, precision=highest)).astype(
        jnp.bfloat16
    )
    seg_rows = tok_rows // tp_count
    own_rows = lax.dynamic_slice_in_dim(tokens, tp_index * seg_rows, seg_rows, 0).astype(
        jnp.float32
    )
    own_logit = lax.dynamic_slice_in_dim(logit_grad, tp_index * seg_rows, seg_rows, 0)
    router_grad = lax.psum_scatter(
        jnp.dot(own_rows.T, own_logit, precision=highest),
        ("ep", "tp"),
        scatter_dimension=0,
        tiled=True,
    )
    return (token_grad, gate_grad, grad_gate[None], grad_up[None], grad_down[None], router_grad)


def solution(mesh):
    placed = (
        P("ep", None),
        P("ep", None),
        P("ep", None),
        P(),
        P("ep", None, "tp"),
        P("ep", None, "tp"),
        P("ep", "tp", None),
    )
    return jax.shard_map(
        shards,
        mesh=mesh,
        in_specs=placed,
        out_specs=(
            P("ep", "tp"),
            P("ep", None),
            P("ep", None, "tp"),
            P("ep", None, "tp"),
            P("ep", "tp", None),
            P(("ep", "tp"), None),
        ),
        check_vma=False,
    )
```

profile of v0, /device:TPU:0, one launch (start us, length us, event | category | flops | bytes accessed | tf_op | source)
XLA Modules:
  0.0 325.1 jit_solution(1084350082928045645)
XLA Ops:
  7.2 0.9 copy.70
  8.2 0.1 eq.109
  8.3 1.2 reduce-window.6
  9.5 0.1 slice.24
  9.6 0.1 copy.71
  9.8 0.7 fusion.37
  10.4 0.1 copy.72
  10.6 0.1 add_add_fusion
  10.7 0.1 copy.73
  10.8 0.1 convert_reduce_fusion.1
  10.9 1.2 convolution_convert_fusion.2
  12.1 27.3 %all_to_all.33 = bf16[8,96,512]{2,1,0:T(8,128)(2,1)} all-to-all(bf16[8,96,512]{2,1,0:T(8,128)(2,1)S(1)} %bitcast.80), channel_id=1, replica_groups=mesh['ep'=8,'tp'=4] {'ep'}, dimensions={0} | all-to-all | bytes 1572864 | tf_op jit(solution)/shard_map/all_to_all | solution.py:99
  39.5 1.2 convolution_convert_fusion.3
  40.8 23.3 %all_to_all.34 = bf16[8,96,512]{2,1,0:T(8,128)(2,1)} all-to-all(bf16[8,96,512]{2,1,0:T(8,128)(2,1)S(1)} %bitcast.81), channel_id=1, replica_groups=mesh['ep'=8,'tp'=4] {'ep'}, dimensions={0} | all-to-all | bytes 1572864 | tf_op jit(solution)/shard_map/all_to_all | solution.py:100
  64.1 0.1 copy.75
  64.2 0.1 eq.116
  64.5 0.2 fusion.45
  64.7 2.4 all-gather.5.cloned.1.call-done
  67.1 5.7 %fusion.11 = f32[768,512]{0,1:T(8,128)} fusion(bf16[768,2048]{1,0:T(8,128)(2,1)} %bitcast.95, bf16[1,2048,512]{2,1,0:T(8,128)(2,1)} %param.12), kind=kOutput, calls=%fused_computation.15 | convolution fusion | flops 1610612736 | bytes 6815744 | tf_op jit(solution)/shard_map/dot_general | solution.py:37
  72.8 3.0 fusion.8
  75.8 21.4 %all-gather.3.cloned.1.call-done = bf16[8,96,2048]{2,1,0:T(8,128)(2,1)} async-done(((bf16[8,96,512]{2,1,0:T(8,128)(2,1)}), bf16[8,96,2048]{2,1,0:T(8,128)(2,1)}) %all-gather.3.cloned.1.call-update) | async-done | bytes 3145744 | tf_op jit(solution)/shard_map/all_gather | solution.py:105
  97.2 6.7 %multiply_reduce_fusion = (f32[768]{0:T(1024)S(1)}, bf16[768,512]{0,1:T(8,128)(2,1)}, f32[768,512]{0,1:T(8,128)}) fusion(f32[768,512]{0,1:T(8,128)} %fusion.11, f32[768,512]{0,1:T(8,128)} %fusion.8, bf16[768,2048]{1,0:T(8,128)(2,1)} %bitcast.99, bf16[1,512,2048]{2,1,0:T(8,128)(2,1)} %param.13), kind=kOutput, calls=%fused_computation.20 | convolution fusion | flops 1614150912 | bytes 10750976 | tf_op jit(solution)/shard_map/dot_general | solution.py:38
  104.1 5.9 %psum.7 = bf16[8,96]{1,0:T(8,128)(2,1)S(1)} all-reduce(f32[8,96]{1,0:T(8,128)S(1)} %reshape.150), channel_id=1, replica_groups=mesh['ep'=8,'tp'=4] {'tp'}, use_global_device_ids=true, to_apply=%region_7.8 | all-reduce | flops 768 | bytes 4608 | tf_op jit(solution)/shard_map/psum | solution.py:126
  109.9 0.6 copy.80
  110.5 5.7 %all-to-all-start.4 = ((bf16[8,1,96]{2,1,0:T(2,128)(2,1)}), bf16[8,1,96]{2,1,0:T(2,128)(2,1)S(1)}, u32[]{:S(2)}, u32[]{:S(2)}) async-start(bf16[8,1,96]{2,1,0:T(2,128)(2,1)} %copy.80), calls=%async_computation.5 | async-start | bytes 8192 | tf_op jit(solution)/shard_map/all_to_all | solution.py:131
  116.3 0.1 copy.78
  116.4 0.1 copy.79
  116.5 6.1 %all-to-all-done.4 = bf16[8,1,96]{2,1,0:T(2,128)(2,1)S(1)} async-done(((bf16[8,1,96]{2,1,0:T(2,128)(2,1)}), bf16[8,1,96]{2,1,0:T(2,128)(2,1)S(1)}, u32[]{:S(2)}, u32[]{:S(2)}) %all-to-all-start.4) | async-done | bytes 1568 | tf_op jit(solution)/shard_map/all_to_all | solution.py:131
  122.6 0.2 fusion.23
  122.9 0.1 copy.76
  123.0 0.2 reshape.155
  123.2 0.2 fusion.21
  123.4 8.9 %all_to_all.35 = bf16[8,1,96]{2,1,0:T(2,128)(2,1)S(1)} all-to-all(bf16[8,1,96]{2,1,0:T(2,128)(2,1)S(1)} %copy.77), channel_id=1, replica_groups=mesh['ep'=8,'tp'=4] {'ep'}, dimensions={0} | all-to-all | bytes 3072 | tf_op jit(solution)/shard_map/all_to_all | solution.py:101
  132.4 3.1 multiply_convert_fusion.7
  135.5 1.8 fusion.6
  137.4 0.3 copy-done.4
  137.7 3.5 %add_convert_fusion = bf16[768,2048]{1,0:T(8,128)(2,1)} fusion(f32[768,2048]{1,0:T(8,128)S(1)} %fusion.6, bf16[768,512]{0,1:T(8,128)(2,1)S(1)} %get-tuple-element.12, bf16[1,2048,512]{2,1,0:T(8,128)(2,1)S(1)} %copy-done.4), kind=kOutput, calls=%fused_computation.1 | convolution fusion | flops 1613758464 | bytes 12320768 | tf_op jit(solution)/shard_map/dot_general | solution.py:117
  141.4 1.8 fusion.31
  143.2 33.2 %reduce-scatter.5.cloned.1.call-done = bf16[8,96,512]{2,1,0:T(8,128)(2,1)} async-done(((bf16[8,96,2048]{2,1,0:T(8,128)(2,1)}), bf16[8,96,512]{2,1,0:T(8,128)(2,1)}) %reduce-scatter.5.cloned.1.call-update) | async-done | bytes 786448 | tf_op jit(solution)/shard_map/reduce_scatter | solution.py:120
  176.4 5.5 %all-to-all-start.3 = ((bf16[8,96,512]{2,1,0:T(8,128)(2,1)}), bf16[8,96,512]{2,1,0:T(8,128)(2,1)S(1)}, u32[]{:S(2)}, u32[]{:S(2)}) async-start(bf16[8,96,512]{2,1,0:T(8,128)(2,1)} %reduce-scatter.5.cloned.1.call-done), calls=%async_computation.4 | async-start | bytes 1572864 | tf_op jit(solution)/shard_map/all_to_all | solution.py:128
  181.9 5.4 %fusion.3 = bf16[1,2048,512]{2,1,0:T(8,128)(2,1)} fusion(bf16[768,2048]{1,0:T(8,128)(2,1)} %bitcast.96, bf16[768,512]{0,1:T(8,128)(2,1)} %copy-done.3), kind=kOutput, calls=%fused_computation.7 | convolution fusion | flops 1611661312 | bytes 6029312 | tf_op jit(solution)/shard_map/dot_general | solution.py:53
  187.3 3.2 fusion.5
  190.6 3.2 fusion.4
  193.8 121.5 %reduce-scatter.7.cloned.1.call-done = f32[64,4]{1,0:T(8,128)} async-done(((f32[2048,4]{1,0:T(8,128)}), f32[64,4]{1,0:T(8,128)}) %reduce-scatter.7.cloned.1.call-update) | async-done | bytes 1040
  315.3 1.4 copy.85
  316.7 0.1 convert_reduce_fusion
  316.9 0.7 convolution_bitcast_fusion
  317.6 1.0 fusion.16
  (57 shorter events, 0.9 us)
Async XLA Ops:
  7.2 65.6 %copy-start = (bf16[1,2048,512]{2,1,0:T(8,128)(2,1)S(1)}, bf16[1,2048,512]{2,1,0:T(8,128)(2,1)}, u32[]{:S(2)}) copy-start(bf16[1,2048,512]{2,1,0:T(8,128)(2,1)} %param.11) | copy-start | bytes 6291460
  7.2 60.0 %all-gather.5.cloned.1.call-start = ((), (), s32[]{:S(2)}) async-start(), calls=%async_computation.8 | async-start | bytes 3932160 | tf_op jit(solution)/shard_map/all_gather | solution.py:104
  39.4 24.9 %copy-start.7 = (s32[128,2]{0,1:T(2,128)S(1)}, s32[128,2]{0,1:T(2,128)}, u32[]{:S(2)}) copy-start(s32[128,2]{0,1:T(2,128)} %param.9) | copy-start | bytes 3076
  39.5 25.0 %copy-start.5 = (bf16[128,2048]{1,0:T(8,128)(2,1)S(1)}, bf16[128,2048]{1,0:T(8,128)(2,1)}, u32[]{:S(2)}) copy-start(bf16[128,2048]{1,0:T(8,128)(2,1)} %param.7) | copy-start | bytes 1572868
  39.5 25.0 %copy-start.6 = (bf16[2048,4]{0,1:T(4,128)(2,1)S(1)}, bf16[2048,4]{0,1:T(4,128)(2,1)}, u32[]{:S(2)}) copy-start(bf16[2048,4]{0,1:T(4,128)(2,1)} %param.10) | copy-start | bytes 49156
  39.5 57.8 %all-gather.3.cloned.1.call-start = ((), (), s32[]{:S(2)}) async-start(), calls=%async_computation.7 | async-start | bytes 3932160 | tf_op jit(solution)/shard_map/all_gather | solution.py:105
  67.1 5.7 %copy-start.9 = (bf16[8,96,2048]{2,1,0:T(8,128)(2,1)S(1)}, bf16[8,96,2048]{2,1,0:T(8,128)(2,1)}, u32[]{:S(2)}) copy-start(bf16[8,96,2048]{2,1,0:T(8,128)(2,1)} %all-gather.5.cloned.1.call-done) | copy-start | bytes 9437188
  110.5 12.1 %all-to-all-start.4 = ((bf16[8,1,96]{2,1,0:T(2,128)(2,1)}), bf16[8,1,96]{2,1,0:T(2,128)(2,1)S(1)}, u32[]{:S(2)}, u32[]{:S(2)}) async-start(bf16[8,1,96]{2,1,0:T(2,128)(2,1)} %copy.80), calls=%async_computation.5 | async-start | bytes 8192 | tf_op jit(solution)/shard_map/all_to_all | solution.py:131
  116.2 60.2 %reduce-scatter.5.cloned.1.call-start = ((), (), s32[]{:S(2)}) async-start(), calls=%async_computation.9 | async-start | bytes 3932160 | tf_op jit(solution)/shard_map/reduce_scatter | solution.py:120
  122.8 12.7 %copy-start.8 = (f32[1,128,2,1]{1,0,3,2:T(1,128)}, f32[1,128,2,1]{1,0,3,2:T(1,128)S(1)}, u32[]{:S(2)}) copy-start(f32[1,128,2,1]{1,0,3,2:T(1,128)S(1)} %fusion.23) | copy-start | bytes 3076
  135.5 1.9 copy-start.3
  135.5 1.9 copy-start.1
  135.5 2.2 copy-start.4
  141.3 174.1 %reduce-scatter.7.cloned.1.call-start = ((), (), s32[]{:S(2)}) async-start(), calls=%async_computation.10 | async-start | bytes 1081344
  176.4 140.3 %all-to-all-start.3 = ((bf16[8,96,512]{2,1,0:T(8,128)(2,1)}), bf16[8,96,512]{2,1,0:T(8,128)(2,1)S(1)}, u32[]{:S(2)}, u32[]{:S(2)}) async-start(bf16[8,96,512]{2,1,0:T(8,128)(2,1)} %reduce-scatter.5.cloned.1.call-done), calls=%async_computation.4 | async-start | bytes 1572864 | tf_op jit(solution)/shard_map/all_to_all | solution.py:128
  181.9 5.4 %copy-start.11 = (bf16[8,96,2048]{2,1,0:T(8,128)(2,1)S(1)}, bf16[8,96,2048]{2,1,0:T(8,128)(2,1)}, u32[]{:S(2)}) copy-start(bf16[8,96,2048]{2,1,0:T(8,128)(2,1)} %all-gather.3.cloned.1.call-done) | copy-start | bytes 9437188
  181.9 5.4 %copy-start.12 = (bf16[768,512]{0,1:T(8,128)(2,1)S(1)}, bf16[768,512]{0,1:T(8,128)(2,1)}, u32[]{:S(2)}) copy-start(bf16[768,512]{0,1:T(8,128)(2,1)} %get-tuple-element.11) | copy-start | bytes 2359300
  187.3 3.3 %copy-start.2 = (bf16[768,512]{0,1:T(8,128)(2,1)S(1)}, bf16[768,512]{0,1:T(8,128)(2,1)}, u32[]{:S(2)}) copy-start(bf16[768,512]{0,1:T(8,128)(2,1)} %copy-done.1) | copy-start | bytes 2359300
  187.3 3.3 %copy-start.10 = (bf16[8,96,2048]{2,1,0:T(8,128)(2,1)S(1)}, bf16[8,96,2048]{2,1,0:T(8,128)(2,1)}, u32[]{:S(2)}) copy-start(bf16[8,96,2048]{2,1,0:T(8,128)(2,1)} %all-gather.5.cloned.1.call-done) | copy-start | bytes 9437188
Sparse Core Ops, SparseCore 0:
  39.6 27.5 all-gather.4
  68.7 28.4 all-gather.2
  141.4 34.9 reduce-scatter.4
  178.5 136.7 reduce-scatter.6
where the time goes:
time: 326 us; the launch traced here: 325 us
  waiting for transfers between devices  185 us (57%)
  blocking collectives  65.4 us (20%)
  matrix products  39.1 us (12%)
  between operations  14 us (4%)
  starting transfers between devices  11.3 us (3%)
  other arithmetic  5.65 us (2%)
  local copies, waits for them, and re-layouts  4.82 us (1%)
    unnamed x5, waiting for transfers between devices  122 us
    reduce_scatter x1, waiting for transfers between devices, shards(): lax.psum_scatter(partial_dx.reshape(ep_count, capacity, width).astype(jnp...  33.2 us
    all_to_all x1, blocking collectives, shards(): lax.all_to_all(pack_rows(tok_part), 'ep', split_axis=0, concat_axis=0, ti...  27.3 us
    all_to_all x1, blocking collectives, shards(): lax.all_to_all(pack_rows(cot_part), 'ep', split_axis=0, concat_axis=0, ti...  23.3 us
    all_gather x1, waiting for transfers between devices, shards(): lax.all_gather(recv_cot_part, 'tp', axis=2, tiled=True)  21.4 us
    all_to_all x1, blocking collectives, shards(): lax.all_to_all(gate_out, 'ep', split_axis=0, concat_axis=0, tiled=True)  8.86 us
    dot_general x1, matrix products, expert_grads(): lax.dot_general(cot_in, down_weight, (((1,), (1,)), ((), ())), preferred_...  6.74 us
  transfers between devices with their start and end apart: 6, of which 5 were waited for; matrix products, arithmetic and copies ran while one was open for 8% of the time, Pallas kernels for 0%

commit v1 on v0

--- a/solution.py
+++ b/solution.py
@@ -158,6 +158,187 @@
     )
     return (token_grad, gate_grad, grad_gate[None], grad_up[None], grad_down[None], router_grad)
 
+def fast_shards(tokens, cotangent, routes, router, w_gate, w_up, w_down):
+    f32, bf16 = jnp.float32, jnp.bfloat16
+    highest = lax.Precision.HIGHEST
+    axes = ("ep", "tp")
+    ep_count = lax.axis_size("ep")
+    tp_count = lax.axis_size("tp")
+    total = ep_count * tp_count
+    experts = ep_count // BLOCKS
+    rows, width = tokens.shape
+    top = routes.shape[1]
+    cap = 3 * rows * top // (2 * experts)
+    quarter = width // tp_count
+    hid = w_gate.shape[2]
+    ep = lax.axis_index("ep")
+    tp = lax.axis_index("tp")
+    here = ep // BLOCKS
+    core = tp % 2
+    pad = 8
+
+    def swap(value, bits):
+        return lax.ppermute(value, axes, [(i, i ^ bits) for i in range(total)])
+
+    def mixed(value, bits_even, bits_odd):
+        return lax.ppermute(
+            value, axes, [(i, i ^ (bits_odd if i % 2 else bits_even)) for i in range(total)]
+        )
+
+    cbit, ybit, xbit, zbit = 1, 2, tp_count, tp_count * BLOCKS
+
+    logits = jnp.dot(tokens, router, preferred_element_type=f32)
+    labels = jnp.arange(experts, dtype=jnp.int32)
+    picked = (routes[:, :, None] == labels[None, None, :]).astype(f32)
+    chosen = jnp.sum(picked * logits[:, None, :], axis=2)
+    margin = chosen[:, 0] - chosen[:, 1]
+    weights = jnp.stack([jax.nn.sigmoid(margin), jax.nn.sigmoid(-margin)], axis=1)
+    product = weights[:, 0] * weights[:, 1]
+    near = here ^ labels
+    hit = jnp.any(routes[None] == near[:, None, None], axis=2)
+    lower = (jnp.arange(rows)[:, None] <= jnp.arange(rows)[None, :]).astype(bf16)
+    rank = jnp.dot(hit.astype(bf16), lower, preferred_element_type=f32).astype(jnp.int32) - 1
+    slots = jnp.arange(cap, dtype=jnp.int32)
+    place = (hit[:, None, :] & (rank[:, None, :] == slots[None, :, None])).astype(bf16)
+    first = routes[None, :, 0] == near[:, None]
+    gate_tok = jnp.where(first, weights[None, :, 0], weights[None, :, 1]).astype(bf16)
+    other_tok = jnp.where(first, routes[None, :, 1], routes[None, :, 0]).astype(bf16)
+    prod_hi = product.astype(bf16)
+    prod_lo = (product - prod_hi.astype(f32)).astype(bf16)
+    flat = jnp.broadcast_to(prod_hi[None], gate_tok.shape), jnp.broadcast_to(prod_lo[None], gate_tok.shape)
+    meta_tok = jnp.stack([gate_tok, flat[0], flat[1], other_tok], axis=1)
+    meta = jnp.einsum("jkt,jct->jkc", meta_tok, place, preferred_element_type=f32).astype(bf16)
+    meta = jnp.pad(meta, ((0, 0), (0, pad - meta.shape[1]), (0, 2 * quarter - cap)))
+    source = jnp.concatenate(
+        [
+            lax.dynamic_slice_in_dim(tokens, tp * quarter, quarter, 1),
+            lax.dynamic_slice_in_dim(cotangent, tp * quarter, quarter, 1),
+        ],
+        axis=1,
+    )
+    packed = jnp.einsum("jct,td->jcd", place, source, preferred_element_type=f32).astype(bf16)
+    packed = jnp.concatenate([packed, meta], axis=1)
+
+    turn = tp ^ jnp.arange(tp_count)
+    wg = w_gate[0].reshape(tp_count, quarter, hid)[turn].reshape(width, hid)
+    wu = w_up[0].reshape(tp_count, quarter, hid)[turn].reshape(width, hid)
+    wd = w_down[0].reshape(hid, tp_count, quarter)[:, turn].reshape(hid, width)
+
+    half = experts // 2
+    pieces = [list(range(half)), list(range(half, experts))]
+    kept, backs = [], [None] * experts
+    for piece in pieces:
+        got = [packed[j] if j == 0 else swap(packed[j], zbit * j) for j in piece]
+        own = jnp.stack(got)
+        side = swap(own, xbit)
+        over = swap(own, ybit)
+        diag = mixed(jnp.where(core == 0, side, over), ybit, xbit)
+        blocks = jnp.stack([own, side, over, diag])
+        twin = swap(blocks, cbit)
+
+        def merge(which):
+            return jnp.stack(
+                [
+                    jnp.concatenate([which(blocks[0]), which(twin[0]), which(blocks[2]), which(twin[2])], axis=-1),
+                    jnp.concatenate([which(blocks[1]), which(twin[1]), which(blocks[3]), which(twin[3])], axis=-1),
+                ]
+            ).reshape(-1, width)
+
+        x_in = merge(lambda v: v[:, :cap, :quarter])
+        c_in = merge(lambda v: v[:, :cap, quarter:])
+        info = jnp.stack([own[:, cap:, :cap], side[:, cap:, :cap]]).astype(f32)
+        info = jnp.transpose(info, (2, 0, 1, 3)).reshape(pad, -1)
+        gate_col = info[0][:, None]
+        prod_col = info[1] + info[2]
+        pre_gate = jnp.dot(x_in, wg, preferred_element_type=f32)
+        pre_up = jnp.dot(x_in, wu, preferred_element_type=f32)
+        back_grad = lax.dot_general(c_in, wd, (((1,), (1,)), ((), ())), preferred_element_type=f32)
+        sig = jax.nn.sigmoid(pre_gate)
+        active = pre_gate * sig
+        hidden = (active * pre_up).astype(bf16)
+        terms = jnp.sum(hidden.astype(f32) * back_grad, axis=1)
+        scaled = gate_col * back_grad
+        d_gate = (scaled * pre_up * sig * (1.0 + pre_gate * (1.0 - sig))).astype(bf16)
+        d_up = (scaled * active).astype(bf16)
+        s_cot = (gate_col * c_in.astype(f32)).astype(bf16)
+        kept.append((x_in, d_gate, d_up, hidden, s_cot))
+        coef = prod_col * terms
+        sign = (labels[None, :] == here).astype(f32) - (
+            labels[None, :].astype(f32) == info[3][:, None]
+        ).astype(f32)
+        lmat = coef[:, None] * sign
+        l_hi = lmat.astype(bf16)
+        l_lo = (lmat - l_hi.astype(f32)).astype(bf16)
+        rr = lax.dot_general(
+            jnp.concatenate([l_hi, l_lo], axis=1), x_in, (((0,), (0,)), ((), ())), preferred_element_type=f32
+        )
+        rr = rr[:experts] + rr[experts:]
+        chunk = width // total
+        target = (ep * tp_count + tp) ^ jnp.arange(total)
+        spot = (tp ^ (target // ep_count)) * ep_count + target % ep_count
+        rr = rr.reshape(experts, total, chunk)[:, spot]
+        rr = jnp.transpose(rr, (1, 0, 2)).reshape(experts, BLOCKS, tp_count, experts * chunk)
+        rr = jnp.transpose(rr, (1, 0, 2, 3))
+        contract = (((1,), (1,)), ((), ()))
+        dx = lax.dot_general(d_gate, wg, contract, preferred_element_type=f32)
+        dx = (dx + lax.dot_general(d_up, wu, contract, preferred_element_type=f32)).astype(bf16)
+        kp = len(piece)
+        dx = dx.reshape(BLOCKS, kp, cap, tp_count, quarter)
+        gt = jnp.broadcast_to(
+            jnp.pad(terms.reshape(BLOCKS, kp, 1, 1, cap), ((0, 0),) * 4 + ((0, quarter - cap),)),
+            (BLOCKS, kp, 1, tp_count, quarter),
+        ).astype(bf16)
+        kept[-1] = kept[-1] + (rr, gt, dx)
+    router_all = sum(k[5] for k in kept)
+    for piece, k in zip(pieces, kept):
+        gt, dx = k[6], k[7]
+        kp = len(piece)
+        rrow = router_all[:, piece[0] : piece[0] + kp][:, :, None]
+        rrow = jnp.pad(rrow, ((0, 0),) * 4 + ((0, quarter - rrow.shape[-1]),)).astype(bf16)
+        extra = jnp.concatenate([gt, rrow, jnp.zeros((BLOCKS, kp, pad - 2, tp_count, quarter), bf16)], axis=2)
+        full = jnp.concatenate([dx, extra], axis=2)
+        full = jnp.transpose(full, (3, 0, 1, 2, 4)).reshape(2, 2, BLOCKS, kp, cap + pad, quarter)
+        gained = swap(full[:, 1], cbit)
+        summed = full[:, 0].astype(f32) + gained.astype(f32)
+        send = jnp.where(core == 0, summed[1], summed[:, 1]).astype(bf16)
+        keep = jnp.where(core == 0, summed[0], summed[:, 0])
+        keep = keep + mixed(send, ybit, xbit).astype(f32)
+        last = keep[0] + mixed(keep[1].astype(bf16), xbit, ybit).astype(f32)
+        last = last.astype(bf16)
+        for n, j in enumerate(piece):
+            backs[j] = last[n] if j == 0 else swap(last[n], zbit * j)
+    contract_rows = (((0,), (0,)), ((), ()))
+
+    def weight_grad(a, b):
+        left = jnp.concatenate([k[a] for k in kept], axis=0)
+        right = jnp.concatenate([k[b] for k in kept], axis=0)
+        return lax.dot_general(left, right, contract_rows, preferred_element_type=f32).astype(bf16)
+
+    grad_gate = weight_grad(0, 1).reshape(tp_count, quarter, hid)[turn].reshape(width, hid)
+    grad_up = weight_grad(0, 2).reshape(tp_count, quarter, hid)[turn].reshape(width, hid)
+    grad_down = weight_grad(3, 4).reshape(hid, tp_count, quarter)[:, turn].reshape(hid, width)
+    back = jnp.stack(backs)
+    routed = lax.dot_general(
+        place.reshape(-1, rows), back[:, :cap].reshape(-1, quarter), contract_rows, preferred_element_type=f32
+    )
+    gate_slot = back[:, cap, :cap]
+    per = jnp.einsum("jc,jct->jt", gate_slot, place, preferred_element_type=f32)
+    gate_grad = jnp.stack(
+        [jnp.sum(jnp.where(routes[None, :, k] == near[:, None], per, 0.0), axis=0) for k in range(top)], axis=1
+    )
+    router_grad = jnp.sum(back[:, cap + 1, : width // total * experts].astype(f32), axis=0)
+    router_grad = router_grad.reshape(experts, width // total).T
+    lead = product * (gate_grad[:, 0] - gate_grad[:, 1])
+    logit_grad = (picked[:, 0] - picked[:, 1]) * lead[:, None]
+    router_cols = lax.dynamic_slice_in_dim(router, tp * quarter, quarter, 0).astype(f32)
+    token_grad = (routed + jnp.dot(logit_grad, router_cols.T, precision=highest)).astype(bf16)
+    return (token_grad, gate_grad, grad_gate[None], grad_up[None], grad_down[None], router_grad)
+
+
+def fits(mesh):
+    experts = mesh.shape["ep"] // BLOCKS
+    return mesh.shape["tp"] == 4 and experts * BLOCKS == mesh.shape["ep"] and experts & (experts - 1) == 0
+
 
 def solution(mesh):
     placed = (
@@ -170,7 +351,7 @@
         P("ep", "tp", None),
     )
     return jax.shard_map(
-        shards,
+        fast_shards if fits(mesh) else shards,
         mesh=mesh,
         in_specs=placed,
         out_specs=(

time: 326 us -> 174 us (0.53)
  waiting for transfers between devices: 185 us -> 35.1 us
  blocking collectives: 65.4 us -> 0 us
  local copies, waits for them, and re-layouts: 4.82 us -> 63.6 us
  starting transfers between devices: 11.3 us -> 23.9 us
  between operations: 14 us -> 1.44 us
  other arithmetic: 5.65 us -> 12.3 us
    unnamed x5 -> x0, waiting for transfers between devices: 122 us -> none
    all_to_all x3 -> x0, blocking collectives: 59.5 us -> none  [the longest x1 27.3 us: shards(): lax.all_to_all(pack_rows(tok_part), 'ep', split_axis=0, concat_axis=0, ti...]
    ppermute x0 -> x20, waiting for transfers between devices: none -> 35.1 us  [the longest x6 19.4 us: mixed(): lax.ppermute(value, axes, [(i, i ^ (bits_odd if i % 2 else bits_even)) fo...]
    reduce_scatter x1 -> x0, waiting for transfers between devices: 33.2 us -> none  [shards(): lax.psum_scatter(partial_dx.reshape(ep_count, capacity, width).astype(jnp...]
    gather x0 -> x10, local copies, waits for them, and re-layouts: none -> 25 us  [the longest x2 6.13 us: fast_shards(): wd = w_down[0].reshape(hid, tp_count, quarter)[:, turn].reshape(hid, width)]
    ppermute x0 -> x20, starting transfers between devices: none -> 23.9 us  [the longest x14 16.3 us: swap(): return lax.ppermute(value, axes, [(i, i ^ bits) for i in range(total)])]
    all_gather x2 -> x0, waiting for transfers between devices: 23.9 us -> none  [the longest x1 21.4 us: shards(): lax.all_gather(recv_cot_part, 'tp', axis=2, tiled=True)]
    unnamed x29 -> x48, local copies, waits for them, and re-layouts: 2.68 us -> 16.3 us
  transfers between devices with their start and end apart: 6 -> 20, of which waited for: 5 -> 8; matrix products, arithmetic and copies ran while one was open for 8% -> 30% of each run, Pallas kernels for 0% -> 0%
where the time goes in v1:
time: 174 us; the launch traced here: 173 us
  local copies, waits for them, and re-layouts  63.6 us (37%)
  matrix products  37 us (21%)
  waiting for transfers between devices  35.1 us (20%)
  starting transfers between devices  23.9 us (14%)
  other arithmetic  12.3 us (7%)
    ppermute x6, waiting for transfers between devices, mixed(): lax.ppermute(value, axes, [(i, i ^ (bits_odd if i % 2 else bits_even)) fo...  19.4 us
    ppermute x14, starting transfers between devices, swap(): return lax.ppermute(value, axes, [(i, i ^ bits) for i in range(total)])  16.3 us
    unnamed x48, local copies, waits for them, and re-layouts  16.3 us
    ppermute x14, waiting for transfers between devices, swap(): return lax.ppermute(value, axes, [(i, i ^ bits) for i in range(total)])  15.7 us
    reshape x4, local copies, waits for them, and re-layouts, fast_shards(): dx = dx.reshape(BLOCKS, kp, cap, tp_count, quarter)  9.97 us
    dot_general x3, matrix products, weight_grad(): lax.dot_general(left, right, contract_rows, preferred_element_type=f32)  9.5 us
    dot_general x2, matrix products, fast_shards(): lax.dot_general(d_up, wu, contract, preferred_element_type=f32)  8.11 us
    ppermute x6, starting transfers between devices, mixed(): lax.ppermute(value, axes, [(i, i ^ (bits_odd if i % 2 else bits_even)) fo...  7.61 us
  transfers between devices with their start and end apart: 20, of which 8 were waited for; matrix products, arithmetic and copies ran while one was open for 30% of the time, Pallas kernels for 0%

profile of v1, /device:TPU:0, one launch (start us, length us, event | category | flops | bytes accessed | tf_op | source)
XLA Modules:
  0.0 173.4 jit_solution(14920599339707066651)
XLA Ops:
  1.5 1.3 fusion.138
  7.9 3.1 %collective-permute-start = (bf16[104,1024]{1,0:T(8,128)(2,1)S(1)}, bf16[104,1024]{1,0:T(8,128)(2,1)S(1)}, u32[]{:S(2)}, u32[]{:S(2)}) collective-permute-start(bf16[104,1024]{1,0:T(8,128)(2,1)S(1)} %get-tuple-element.57), channel_id=1, source_target_pairs={{0,8},{1,9},{2,10},{3,11},{4,12},{5,13},{6,14},{7,15},{8,0},{9,1},... | collective-permute-start | bytes 638984 | tf_op jit(solution)/shard_map/ppermute | solution.py:181
  11.0 2.5 %collective-permute-start.6 = (bf16[104,1024]{1,0:T(8,128)(2,1)}, bf16[104,1024]{1,0:T(8,128)(2,1)S(1)}, u32[]{:S(2)}, u32[]{:S(2)}) collective-permute-start(bf16[104,1024]{1,0:T(8,128)(2,1)} %get-tuple-element.56), channel_id=1, source_target_pairs={{0,24},{1,25},{2,26},{3,27},{4,28},{5,29},{6,30},{7,31},{8,16},{9,... | collective-permute-start | bytes 638984 | tf_op jit(solution)/shard_map/ppermute | solution.py:181
  13.6 2.0 %gather_fusion.1 = bf16[4,512,512]{2,1,0:T(8,128)(2,1)} fusion(bf16[4,512,512]{2,1,0:T(8,128)(2,1)S(1)} %bitcast.249, s32[1024]{0:T(1024)S(1)} %pad_clamp_fusion.1), kind=kCustom, calls=%fused_computation.1 | custom fusion | bytes 4194320 | tf_op jit(solution)/shard_map/gather | solution.py:224
  15.6 3.7 %gather_fusion.2 = bf16[4,512,512]{2,1,0:T(8,128)(2,1)} fusion(bf16[4,512,512]{2,1,0:T(8,128)(2,1)} %bitcast.281, s32[1024]{0:T(1024)S(1)} %pad_clamp_fusion.1), kind=kCustom, calls=%fused_computation.2 | custom fusion | bytes 4194320 | tf_op jit(solution)/shard_map/gather | solution.py:223
  19.4 2.5 %copy.73 = bf16[1,512,2048]{1,2,0:T(8,128)(2,1)} copy(bf16[1,512,2048]{2,1,0:T(8,128)(2,1)S(1)} %copy-done.11) | data formatting | bytes 4194304 | tf_op args[6]
  21.9 2.8 %copy.74 = bf16[512,4,512]{2,0,1:T(8,128)(2,1)S(1)} copy(bf16[512,4,512]{0,2,1:T(8,128)(2,1)} %bitcast.262) | data formatting | bytes 4194304 | tf_op jit(solution)/shard_map/reshape;squeeze | solution.py:225
  24.7 2.0 %gather_fusion = bf16[4,512,512]{2,1,0:T(8,128)(2,1)} fusion(bf16[512,4,512]{2,0,1:T(8,128)(2,1)S(1)} %copy.74, s32[1024]{0:T(1024)S(1)} %pad_clamp_fusion.1), kind=kCustom, calls=%fused_computation | custom fusion | bytes 4194320 | tf_op jit(solution)/shard_map/gather | solution.py:225
  26.7 4.1 %copy.75 = bf16[512,4,512]{0,2,1:T(8,128)(2,1)} copy(bf16[512,4,512]{2,0,1:T(8,128)(2,1)} %bitcast.260) | data formatting | bytes 4194304 | tf_op jit(solution)/shard_map/gather | solution.py:225
  31.0 1.6 collective-permute-start.1
  32.5 1.5 collective-permute-start.2
  37.2 6.6 %collective-permute-done.1 = bf16[2,104,1024]{2,1,0:T(8,128)(2,1)S(1)} collective-permute-done((bf16[2,104,1024]{2,1,0:T(8,128)(2,1)S(1)}, bf16[2,104,1024]{2,1,0:T(8,128)(2,1)S(1)}, u32[]{:S(2)}, u32[]{:S(2)}) %collective-permute-start.1) | collective-permute-done | bytes 426016 | tf_op jit(solution)/shard_map/ppermute | solution.py:181
  43.7 1.5 collective-permute-done.2
  46.1 1.5 collective-permute-start.3
  47.6 5.3 %collective-permute-done.7 = bf16[2,104,1024]{2,1,0:T(8,128)(2,1)S(1)} collective-permute-done((bf16[2,104,1024]{2,1,0:T(8,128)(2,1)S(1)}, bf16[2,104,1024]{2,1,0:T(8,128)(2,1)S(1)}, u32[]{:S(2)}, u32[]{:S(2)}) %collective-permute-start.7) | collective-permute-done | bytes 426016 | tf_op jit(solution)/shard_map/ppermute | solution.py:181
  52.9 1.6 collective-permute-start.9
  54.5 7.0 %collective-permute-done.9 = bf16[2,104,1024]{2,1,0:T(8,128)(2,1)S(1)} collective-permute-done((bf16[2,104,1024]{2,1,0:T(8,128)(2,1)S(1)}, bf16[2,104,1024]{2,1,0:T(8,128)(2,1)S(1)}, u32[]{:S(2)}, u32[]{:S(2)}) %collective-permute-start.9) | collective-permute-done | bytes 426016 | tf_op jit(solution)/shard_map/ppermute | solution.py:184
  61.5 1.4 pad_maximum_fusion.4
  64.5 2.4 %collective-permute-done.10 = bf16[4,2,104,1024]{3,2,1,0:T(8,128)(2,1)} collective-permute-done((bf16[4,2,104,1024]{3,2,1,0:T(8,128)(2,1)}, bf16[4,2,104,1024]{3,2,1,0:T(8,128)(2,1)}, u32[]{:S(2)}, u32[]{:S(2)}) %collective-permute-start.10) | collective-permute-done | bytes 1703968 | tf_op jit(solution)/shard_map/ppermute | solution.py:181
  66.9 1.6 slice_bitcast_fusion.13
  68.9 2.0 %copy-done.2 = bf16[4,512,512]{2,1,0:T(8,128)(2,1)S(1)} copy-done((bf16[4,512,512]{2,1,0:T(8,128)(2,1)S(1)}, bf16[4,512,512]{2,1,0:T(8,128)(2,1)}, u32[]{:S(2)}) %copy-start.2) | copy-done | bytes 2097176
  78.0 2.0 %copy-done.12 = bf16[512,4,512]{0,2,1:T(8,128)(2,1)S(1)} copy-done((bf16[512,4,512]{0,2,1:T(8,128)(2,1)S(1)}, bf16[512,4,512]{0,2,1:T(8,128)(2,1)}, u32[]{:S(2)}) %copy-start.12) | copy-done | bytes 2097176
  80.0 2.1 %multiply_reduce_fusion.1 = (f32[384]{0:T(512)S(1)}, bf16[384,512]{1,0:T(8,128)(2,1)}, bf16[384,512]{1,0:T(8,128)(2,1)S(1)}, bf16[384,512]{1,0:T(8,128)(2,1)S(1)}) fusion(f32[384,512]{1,0:T(8,128)S(1)} %fusion.139, f32[384,512]{1,0:T(8,128)S(1)} %fusion.140, f32[384]{0:T(512)S(1)} %mul.166, bf16[384,2048]{1,0:T(8,128)(2,1)S(1)} %bitcast.275, ...), kind=kOutput, calls=%fused_computation.91 | convolution fusion | flops 809041536 | bytes 6425600 | tf_op jit(solution)/shard_map/dot_general | solution.py:255
  82.1 2.7 %fusion.141 = f32[384,2048]{1,0:T(8,128)} fusion(bf16[384,512]{1,0:T(8,128)(2,1)S(1)} %get-tuple-element.39, bf16[2048,512]{1,0:T(8,128)(2,1)S(1)} %bitcast.256), kind=kOutput, calls=%fused_computation.287 | convolution fusion | flops 805306368 | bytes 5636096 | tf_op jit(solution)/shard_map/dot_general | solution.py:283
  85.9 2.0 %multiply_reduce_fusion = (f32[384]{0:T(512)S(1)}, bf16[384,512]{1,0:T(8,128)(2,1)}, bf16[384,512]{1,0:T(8,128)(2,1)S(1)}, bf16[384,512]{1,0:T(8,128)(2,1)S(1)}) fusion(f32[384,512]{1,0:T(8,128)S(1)} %fusion.143, f32[384,512]{1,0:T(8,128)S(1)} %fusion.142, f32[384]{0:T(512)S(1)} %mul.188, bf16[384,2048]{1,0:T(8,128)(2,1)S(1)} %bitcast.276, ...), kind=kOutput, calls=%fused_computation.87 | convolution fusion | flops 809041536 | bytes 6425600 | tf_op jit(solution)/shard_map/dot_general | solution.py:255
  87.9 2.6 %fusion.144 = f32[384,2048]{1,0:T(8,128)} fusion(bf16[384,512]{1,0:T(8,128)(2,1)S(1)} %get-tuple-element.40, bf16[2048,512]{1,0:T(8,128)(2,1)S(1)} %bitcast.257), kind=kOutput, calls=%fused_computation.290 | convolution fusion | flops 805306368 | bytes 5636096 | tf_op jit(solution)/shard_map/dot_general | solution.py:283
  90.6 3.2 %convolution_convert_fusion.1 = bf16[2048,512]{1,0:T(8,128)(2,1)} fusion(bf16[384,2048]{1,0:T(8,128)(2,1)S(1)} %bitcast.267, bf16[384,2048]{1,0:T(8,128)(2,1)S(1)} %bitcast.272, bf16[384,512]{1,0:T(8,128)(2,1)S(1)} %get-tuple-element.40, bf16[384,512]{1,0:T(8,128)(2,1)S(1)} %get-tuple-element.39), kind=kOutput, calls=%fused_computation.22 | convolution fusion | flops 1619525632 | bytes 6029312 | tf_op jit(solution)/shard_map/dot_general | solution.py:315
  93.7 1.5 multiply_convert_fusion
  95.8 1.7 fusion.69
  99.4 4.0 %add_convert_fusion.1 = bf16[384,2048]{1,0:T(8,128)(2,1)} fusion(f32[384,2048]{1,0:T(8,128)} %fusion.141, bf16[384,512]{1,0:T(8,128)(2,1)S(1)} %get-tuple-element.53, bf16[2048,512]{1,0:T(8,128)(2,1)S(1)} %bitcast.252), kind=kOutput, calls=%fused_computation.19 | convolution fusion | flops 806879232 | bytes 7208960 | tf_op jit(solution)/shard_map/dot_general | solution.py:284
  103.5 3.9 %reshape.529 = bf16[2,2,96,4,512]{4,3,2,1,0:T(4,128)(2,1)} reshape(bf16[384,2048]{1,0:T(8,128)(2,1)} %add_convert_fusion.1) | data formatting | bytes 3145728 | tf_op jit(solution)/shard_map/reshape | solution.py:286
  107.3 2.9 %copy.78 = bf16[2,2,96,4,512]{4,2,1,0,3:T(8,128)(2,1)} copy(bf16[2,2,96,4,512]{4,3,2,1,0:T(4,128)(2,1)} %reshape.529) | data formatting | bytes 3145728 | tf_op jit(solution)/shard_map/reshape | solution.py:286
  110.3 4.1 %add_convert_fusion = bf16[384,2048]{1,0:T(8,128)(2,1)} fusion(f32[384,2048]{1,0:T(8,128)} %fusion.144, bf16[384,512]{1,0:T(8,128)(2,1)S(1)} %get-tuple-element.54, bf16[2048,512]{1,0:T(8,128)(2,1)S(1)} %bitcast.253), kind=kOutput, calls=%fused_computation.18 | convolution fusion | flops 806879232 | bytes 7208960 | tf_op jit(solution)/shard_map/dot_general | solution.py:284
  114.4 2.9 %reshape.536 = bf16[2,2,96,4,512]{4,3,2,1,0:T(4,128)(2,1)S(1)} reshape(bf16[384,2048]{1,0:T(8,128)(2,1)} %add_convert_fusion) | data formatting | bytes 3145728 | tf_op jit(solution)/shard_map/reshape | solution.py:286
  122.8 3.2 %convolution_convert_fusion = bf16[2048,512]{1,0:T(8,128)(2,1)} fusion(bf16[384,2048]{1,0:T(8,128)(2,1)S(1)} %bitcast.269, bf16[384,2048]{1,0:T(8,128)(2,1)S(1)} %bitcast.274, bf16[384,512]{1,0:T(8,128)(2,1)S(1)} %get-tuple-element.54, bf16[384,512]{1,0:T(8,128)(2,1)S(1)} %get-tuple-element.53), kind=kOutput, calls=%fused_computation.21 | convolution fusion | flops 1619525632 | bytes 6029312 | tf_op jit(solution)/shard_map/dot_general | solution.py:315
  126.3 1.6 collective-permute-start.16
  128.8 5.7 %collective-permute-done.16 = bf16[2,2,104,512]{3,2,1,0:T(8,128)(2,1)S(1)} collective-permute-done((bf16[2,2,104,512]{3,2,1,0:T(8,128)(2,1)S(1)}, bf16[2,2,104,512]{3,2,1,0:T(8,128)(2,1)S(1)}, u32[]{:S(2)}, u32[]{:S(2)}) %collective-permute-start.16) | collective-permute-done | bytes 426016 | tf_op jit(solution)/shard_map/ppermute | solution.py:184
  135.9 5.4 %collective-permute-done.12 = bf16[2,2,104,512]{3,2,1,0:T(8,128)(2,1)S(1)} collective-permute-done((bf16[2,2,104,512]{3,2,1,0:T(8,128)(2,1)S(1)}, bf16[2,2,104,512]{3,2,1,0:T(8,128)(2,1)S(1)}, u32[]{:S(2)}, u32[]{:S(2)}) %collective-permute-start.12) | collective-permute-done | bytes 426016 | tf_op jit(solution)/shard_map/ppermute | solution.py:184
  142.8 3.0 %collective-permute-start.19 = (bf16[104,512]{1,0:T(8,128)(2,1)S(1)}, bf16[104,512]{1,0:T(8,128)(2,1)S(1)}, u32[]{:S(2)}, u32[]{:S(2)}) collective-permute-start(bf16[104,512]{1,0:T(8,128)(2,1)S(1)} %get-tuple-element.98), channel_id=1, source_target_pairs={{0,24},{1,25},{2,26},{3,27},{4,28},{5,29},{6,30},{7,31},{8,16},{9,... | collective-permute-start | bytes 319496 | tf_op jit(solution)/shard_map/ppermute | solution.py:181
  146.1 1.3 collective-permute-done.13
  147.5 1.6 collective-permute-start.14
  149.1 3.2 %fusion.5 = bf16[512,2048]{1,0:T(8,128)(2,1)} fusion(bf16[384,2048]{1,0:T(8,128)(2,1)S(1)} %copy-done.14, bf16[384,2048]{1,0:T(8,128)(2,1)S(1)} %multiply_convert_fusion.1, bf16[384,512]{1,0:T(8,128)(2,1)S(1)} %copy-done.20, bf16[384,512]{1,0:T(8,128)(2,1)S(1)} %copy-done.19), kind=kOutput, calls=%fused_computation.20 | convolution fusion | flops 1619525632 | bytes 6029312 | tf_op jit(solution)/shard_map/dot_general | solution.py:315
  152.3 2.0 %gather_fusion.5 = bf16[4,512,512]{2,1,0:T(8,128)(2,1)} fusion(bf16[4,512,512]{2,1,0:T(8,128)(2,1)S(1)} %bitcast.284, s32[1024]{0:T(1024)S(1)} %pad_clamp_fusion.1), kind=kCustom, calls=%fused_computation.5 | custom fusion | bytes 4194320 | tf_op jit(solution)/shard_map/gather | solution.py:317
  154.3 3.6 %gather_fusion.6 = bf16[4,512,512]{2,1,0:T(8,128)(2,1)} fusion(bf16[4,512,512]{2,1,0:T(8,128)(2,1)} %bitcast.285, s32[1024]{0:T(1024)S(1)} %pad_clamp_fusion.1), kind=kCustom, calls=%fused_computation.6 | custom fusion | bytes 4194320 | tf_op jit(solution)/shard_map/gather | solution.py:318
  157.8 1.8 %copy.109 = bf16[64,4,8,512]{3,2,0,1:T(8,128)(2,1)S(1)} copy(bf16[64,4,8,512]{3,2,1,0:T(8,128)(2,1)} %bitcast.288) | data formatting | bytes 4194304 | tf_op jit(solution)/shard_map/reshape | solution.py:319
  159.6 2.0 %gather_fusion.7 = bf16[4,512,512]{2,1,0:T(8,128)(2,1)} fusion(bf16[512,4,512]{2,0,1:T(8,128)(2,1)S(1)} %bitcast.258, s32[1024]{0:T(1024)S(1)} %pad_clamp_fusion.1), kind=kCustom, calls=%fused_computation.7 | custom fusion | bytes 4194320 | tf_op jit(solution)/shard_map/gather | solution.py:319
  161.6 4.1 %copy.88 = bf16[512,4,512]{0,2,1:T(8,128)(2,1)} copy(bf16[512,4,512]{2,0,1:T(8,128)(2,1)} %bitcast.259) | data formatting | bytes 4194304 | tf_op jit(solution)/shard_map/gather | solution.py:319
  165.8 4.1 %copy.89 = bf16[1,512,2048]{2,1,0:T(8,128)(2,1)} copy(bf16[1,512,2048]{1,2,0:T(8,128)(2,1)} %bitcast.261) | data formatting | bytes 4194304
  (187 shorter events, 36.2 us)
Async XLA Ops:
  0.6 13.0 %copy-start = (bf16[1,2048,512]{2,1,0:T(8,128)(2,1)S(1)}, bf16[1,2048,512]{2,1,0:T(8,128)(2,1)}, u32[]{:S(2)}) copy-start(bf16[1,2048,512]{2,1,0:T(8,128)(2,1)} %param.12) | copy-start | bytes 6291460
  7.0 6.6 %copy-start.18 = (s32[128,2]{0,1:T(2,128)S(1)}, s32[128,2]{0,1:T(2,128)}, u32[]{:S(2)}) copy-start(s32[128,2]{0,1:T(2,128)} %param.9) | copy-start | bytes 3076
  7.9 23.0 %collective-permute-start = (bf16[104,1024]{1,0:T(8,128)(2,1)S(1)}, bf16[104,1024]{1,0:T(8,128)(2,1)S(1)}, u32[]{:S(2)}, u32[]{:S(2)}) collective-permute-start(bf16[104,1024]{1,0:T(8,128)(2,1)S(1)} %get-tuple-element.57), channel_id=1, source_target_pairs={{0,8},{1,9},{2,10},{3,11},{4,12},{5,13},{6,14},{7,15},{8,0},{9,1},... | collective-permute-start | bytes 638984 | tf_op jit(solution)/shard_map/ppermute | solution.py:181
  11.0 23.1 %collective-permute-start.6 = (bf16[104,1024]{1,0:T(8,128)(2,1)}, bf16[104,1024]{1,0:T(8,128)(2,1)S(1)}, u32[]{:S(2)}, u32[]{:S(2)}) collective-permute-start(bf16[104,1024]{1,0:T(8,128)(2,1)} %get-tuple-element.56), channel_id=1, source_target_pairs={{0,24},{1,25},{2,26},{3,27},{4,28},{5,29},{6,30},{7,31},{8,16},{9,... | collective-permute-start | bytes 638984 | tf_op jit(solution)/shard_map/ppermute | solution.py:181
  13.5 20.6 %collective-permute-start.5 = (bf16[104,1024]{1,0:T(8,128)(2,1)}, bf16[104,1024]{1,0:T(8,128)(2,1)S(1)}, u32[]{:S(2)}, u32[]{:S(2)}) collective-permute-start(bf16[104,1024]{1,0:T(8,128)(2,1)} %get-tuple-element.55), channel_id=1, source_target_pairs={{0,16},{1,17},{2,18},{3,19},{4,20},{5,21},{6,22},{7,23},{8,24},{9,... | collective-permute-start | bytes 638984 | tf_op jit(solution)/shard_map/ppermute | solution.py:181
  15.6 3.7 %copy-start.11 = (bf16[1,512,2048]{2,1,0:T(8,128)(2,1)S(1)}, bf16[1,512,2048]{2,1,0:T(8,128)(2,1)}, u32[]{:S(2)}) copy-start(bf16[1,512,2048]{2,1,0:T(8,128)(2,1)} %param.13) | copy-start | bytes 6291460
  31.0 12.8 %collective-permute-start.1 = (bf16[2,104,1024]{2,1,0:T(8,128)(2,1)S(1)}, bf16[2,104,1024]{2,1,0:T(8,128)(2,1)S(1)}, u32[]{:S(2)}, u32[]{:S(2)}) collective-permute-start(bf16[2,104,1024]{2,1,0:T(8,128)(2,1)S(1)} %get-tuple-element.94), channel_id=1, source_target_pairs={{0,4},{1,5},{2,6},{3,7},{4,0},{5,1},{6,2},{7,3},{8,12},{9,13},{10,... | collective-permute-start | bytes 1277960 | tf_op jit(solution)/shard_map/ppermute | solution.py:181
  32.5 12.7 %collective-permute-start.2 = (bf16[2,104,1024]{2,1,0:T(8,128)(2,1)S(1)}, bf16[2,104,1024]{2,1,0:T(8,128)(2,1)S(1)}, u32[]{:S(2)}, u32[]{:S(2)}) collective-permute-start(bf16[2,104,1024]{2,1,0:T(8,128)(2,1)S(1)} %get-tuple-element.94), channel_id=1, source_target_pairs={{0,2},{1,3},{2,0},{3,1},{4,6},{5,7},{6,4},{7,5},{8,10},{9,11},{10,... | collective-permute-start | bytes 1277960 | tf_op jit(solution)/shard_map/ppermute | solution.py:181
  34.1 18.7 %collective-permute-start.7 = (bf16[2,104,1024]{2,1,0:T(8,128)(2,1)S(1)}, bf16[2,104,1024]{2,1,0:T(8,128)(2,1)S(1)}, u32[]{:S(2)}, u32[]{:S(2)}) collective-permute-start(bf16[2,104,1024]{2,1,0:T(8,128)(2,1)S(1)} %get-tuple-element.76), channel_id=1, source_target_pairs={{0,4},{1,5},{2,6},{3,7},{4,0},{5,1},{6,2},{7,3},{8,12},{9,13},{10,... | collective-permute-start | bytes 1277960 | tf_op jit(solution)/shard_map/ppermute | solution.py:181
  34.7 18.1 %collective-permute-start.8 = (bf16[2,104,1024]{2,1,0:T(8,128)(2,1)S(1)}, bf16[2,104,1024]{2,1,0:T(8,128)(2,1)S(1)}, u32[]{:S(2)}, u32[]{:S(2)}) collective-permute-start(bf16[2,104,1024]{2,1,0:T(8,128)(2,1)S(1)} %get-tuple-element.76), channel_id=1, source_target_pairs={{0,2},{1,3},{2,0},{3,1},{4,6},{5,7},{6,4},{7,5},{8,10},{9,11},{10,... | collective-permute-start | bytes 1277960 | tf_op jit(solution)/shard_map/ppermute | solution.py:181
  46.1 17.6 %collective-permute-start.3 = (bf16[2,104,1024]{2,1,0:T(8,128)(2,1)}, bf16[2,104,1024]{2,1,0:T(8,128)(2,1)S(1)}, u32[]{:S(2)}, u32[]{:S(2)}) collective-permute-start(bf16[2,104,1024]{2,1,0:T(8,128)(2,1)} %broadcast_select_fusion.1), channel_id=1, source_target_pairs={{0,2},{1,5},{2,0},{3,7},{4,6},{5,1},{6,4},{7,3},{8,10},{9,13},{10,... | collective-permute-start | bytes 1277960 | tf_op jit(solution)/shard_map/ppermute | solution.py:184
  52.9 8.6 %collective-permute-start.9 = (bf16[2,104,1024]{2,1,0:T(8,128)(2,1)S(1)}, bf16[2,104,1024]{2,1,0:T(8,128)(2,1)S(1)}, u32[]{:S(2)}, u32[]{:S(2)}) collective-permute-start(bf16[2,104,1024]{2,1,0:T(8,128)(2,1)S(1)} %broadcast_select_fusion), channel_id=1, source_target_pairs={{0,2},{1,5},{2,0},{3,7},{4,6},{5,1},{6,4},{7,3},{8,10},{9,13},{10,... | collective-permute-start | bytes 1277960 | tf_op jit(solution)/shard_map/ppermute | solution.py:184
  62.9 3.9 %collective-permute-start.10 = (bf16[4,2,104,1024]{3,2,1,0:T(8,128)(2,1)}, bf16[4,2,104,1024]{3,2,1,0:T(8,128)(2,1)}, u32[]{:S(2)}, u32[]{:S(2)}) collective-permute-start(bf16[4,2,104,1024]{3,2,1,0:T(8,128)(2,1)} %pad_maximum_fusion.4), channel_id=1, source_target_pairs={{0,1},{1,0},{2,3},{3,2},{4,5},{5,4},{6,7},{7,6},{8,9},{9,8},{10,11... | collective-permute-start | bytes 5111816 | tf_op jit(solution)/shard_map/ppermute | solution.py:181
  63.9 9.6 %collective-permute-start.4 = (bf16[4,2,104,1024]{3,2,1,0:T(8,128)(2,1)S(1)}, bf16[4,2,104,1024]{3,2,1,0:T(8,128)(2,1)S(1)}, u32[]{:S(2)}, u32[]{:S(2)}) collective-permute-start(bf16[4,2,104,1024]{3,2,1,0:T(8,128)(2,1)S(1)} %pad_maximum_fusion.3), channel_id=1, source_target_pairs={{0,1},{1,0},{2,3},{3,2},{4,5},{5,4},{6,7},{7,6},{8,9},{9,8},{10,11... | collective-permute-start | bytes 5111816 | tf_op jit(solution)/shard_map/ppermute | solution.py:181
  68.7 2.2 %copy-start.2 = (bf16[4,512,512]{2,1,0:T(8,128)(2,1)S(1)}, bf16[4,512,512]{2,1,0:T(8,128)(2,1)}, u32[]{:S(2)}) copy-start(bf16[4,512,512]{2,1,0:T(8,128)(2,1)} %gather_fusion.1) | copy-start | bytes 6291460
  68.9 21.7 %copy-start.4 = (bf16[2,2,96,2048]{3,2,1,0:T(8,128)(2,1)}, bf16[2,2,96,2048]{3,2,1,0:T(8,128)(2,1)S(1)}, u32[]{:S(2)}) copy-start(bf16[2,2,96,2048]{3,2,1,0:T(8,128)(2,1)S(1)} %pad_maximum_fusion.7) | copy-start | bytes 4718596
  70.9 1.6 copy-start.3
  73.7 0.9 copy-start.17
  74.8 20.5 %copy-start.6 = (bf16[2,2,96,2048]{3,2,1,0:T(8,128)(2,1)}, bf16[2,2,96,2048]{3,2,1,0:T(8,128)(2,1)S(1)}, u32[]{:S(2)}) copy-start(bf16[2,2,96,2048]{3,2,1,0:T(8,128)(2,1)S(1)} %pad_maximum_fusion.6) | copy-start | bytes 4718596
  76.8 0.9 copy-start.16
  77.8 2.2 %copy-start.12 = (bf16[512,4,512]{0,2,1:T(8,128)(2,1)S(1)}, bf16[512,4,512]{0,2,1:T(8,128)(2,1)}, u32[]{:S(2)}) copy-start(bf16[512,4,512]{0,2,1:T(8,128)(2,1)} %copy.75) | copy-start | bytes 6291460
  78.0 4.1 %copy-start.8 = (bf16[2,2,96,2048]{3,2,1,0:T(8,128)(2,1)}, bf16[2,2,96,2048]{3,2,1,0:T(8,128)(2,1)S(1)}, u32[]{:S(2)}) copy-start(bf16[2,2,96,2048]{3,2,1,0:T(8,128)(2,1)S(1)} %pad_maximum_fusion.5) | copy-start | bytes 4718596
  84.8 0.9 copy-start.15
  117.3 1.4 copy-start.10
  120.1 5.9 %collective-permute-start.15 = (bf16[2,2,2,104,512]{4,3,2,0,1:T(8,128)(2,1)S(1)}, bf16[2,2,2,104,512]{4,3,2,0,1:T(8,128)(2,1)S(1)}, u32[]{:S(2)}, u32[]{:S(2)}) collective-permute-start(bf16[2,2,2,104,512]{4,3,2,0,1:T(8,128)(2,1)S(1)} %bitcast.310), channel_id=1, source_target_pairs={{0,1},{1,0},{2,3},{3,2},{4,5},{5,4},{6,7},{7,6},{8,9},{9,8},{10,11... | collective-permute-start | bytes 2555912 | tf_op jit(solution)/shard_map/ppermute | solution.py:181
  120.4 1.4 copy-start.9
  120.5 1.8 %copy-start.5 = (bf16[2,2,96,2048]{3,2,1,0:T(8,128)(2,1)S(1)}, bf16[2,2,96,2048]{3,2,1,0:T(8,128)(2,1)}, u32[]{:S(2)}) copy-start(bf16[2,2,96,2048]{3,2,1,0:T(8,128)(2,1)} %copy-done.4) | copy-start | bytes 4718596
  120.5 2.3 %copy-start.7 = (bf16[2,2,96,2048]{3,2,1,0:T(8,128)(2,1)S(1)}, bf16[2,2,96,2048]{3,2,1,0:T(8,128)(2,1)}, u32[]{:S(2)}) copy-start(bf16[2,2,96,2048]{3,2,1,0:T(8,128)(2,1)} %copy-done.6) | copy-start | bytes 4718596
  120.5 7.4 %collective-permute-start.11 = (bf16[2,2,2,104,512]{4,3,2,0,1:T(8,128)(2,1)S(1)}, bf16[2,2,2,104,512]{4,3,2,0,1:T(8,128)(2,1)S(1)}, u32[]{:S(2)}, u32[]{:S(2)}) collective-permute-start(bf16[2,2,2,104,512]{4,3,2,0,1:T(8,128)(2,1)S(1)} %bitcast.309), channel_id=1, source_target_pairs={{0,1},{1,0},{2,3},{3,2},{4,5},{5,4},{6,7},{7,6},{8,9},{9,8},{10,11... | collective-permute-start | bytes 2555912 | tf_op jit(solution)/shard_map/ppermute | solution.py:181
  126.3 8.2 %collective-permute-start.16 = (bf16[2,2,104,512]{3,2,1,0:T(8,128)(2,1)S(1)}, bf16[2,2,104,512]{3,2,1,0:T(8,128)(2,1)S(1)}, u32[]{:S(2)}, u32[]{:S(2)}) collective-permute-start(bf16[2,2,104,512]{3,2,1,0:T(8,128)(2,1)S(1)} %fusion.20), channel_id=1, source_target_pairs={{0,2},{1,5},{2,0},{3,7},{4,6},{5,1},{6,4},{7,3},{8,10},{9,13},{10,... | collective-permute-start | bytes 1277960 | tf_op jit(solution)/shard_map/ppermute | solution.py:184
  128.2 13.0 %collective-permute-start.12 = (bf16[2,2,104,512]{3,2,1,0:T(8,128)(2,1)S(1)}, bf16[2,2,104,512]{3,2,1,0:T(8,128)(2,1)S(1)}, u32[]{:S(2)}, u32[]{:S(2)}) collective-permute-start(bf16[2,2,104,512]{3,2,1,0:T(8,128)(2,1)S(1)} %fusion.24), channel_id=1, source_target_pairs={{0,2},{1,5},{2,0},{3,7},{4,6},{5,1},{6,4},{7,3},{8,10},{9,13},{10,... | collective-permute-start | bytes 1277960 | tf_op jit(solution)/shard_map/ppermute | solution.py:184
  134.7 8.0 %collective-permute-start.17 = (bf16[2,104,512]{2,1,0:T(8,128)(2,1)S(1)}, bf16[2,104,512]{2,1,0:T(8,128)(2,1)S(1)}, u32[]{:S(2)}, u32[]{:S(2)}) collective-permute-start(bf16[2,104,512]{2,1,0:T(8,128)(2,1)S(1)} %fusion.46), channel_id=1, source_target_pairs={{0,4},{1,3},{2,6},{3,1},{4,0},{5,7},{6,2},{7,5},{8,12},{9,11},{10,... | collective-permute-start | bytes 638984 | tf_op jit(solution)/shard_map/ppermute | solution.py:184
  141.4 7.6 %copy-start.14 = (bf16[384,2048]{1,0:T(8,128)(2,1)S(1)}, bf16[384,2048]{1,0:T(8,128)(2,1)}, u32[]{:S(2)}) copy-start(bf16[384,2048]{1,0:T(8,128)(2,1)} %multiply_convert_fusion) | copy-start | bytes 4718596
  141.4 7.6 %copy-start.19 = (bf16[384,512]{1,0:T(8,128)(2,1)S(1)}, bf16[384,512]{1,0:T(8,128)(2,1)}, u32[]{:S(2)}) copy-start(bf16[384,512]{1,0:T(8,128)(2,1)} %get-tuple-element.35) | copy-start | bytes 1179652
  141.5 7.6 %copy-start.20 = (bf16[384,512]{1,0:T(8,128)(2,1)S(1)}, bf16[384,512]{1,0:T(8,128)(2,1)}, u32[]{:S(2)}) copy-start(bf16[384,512]{1,0:T(8,128)(2,1)} %get-tuple-element.33) | copy-start | bytes 1179652
  141.5 5.9 %collective-permute-start.13 = (bf16[2,104,512]{2,1,0:T(8,128)(2,1)S(1)}, bf16[2,104,512]{2,1,0:T(8,128)(2,1)S(1)}, u32[]{:S(2)}, u32[]{:S(2)}) collective-permute-start(bf16[2,104,512]{2,1,0:T(8,128)(2,1)S(1)} %fusion.45), channel_id=1, source_target_pairs={{0,4},{1,3},{2,6},{3,1},{4,0},{5,7},{6,2},{7,5},{8,12},{9,11},{10,... | collective-permute-start | bytes 638984 | tf_op jit(solution)/shard_map/ppermute | solution.py:184
  142.8 27.1 %collective-permute-start.19 = (bf16[104,512]{1,0:T(8,128)(2,1)S(1)}, bf16[104,512]{1,0:T(8,128)(2,1)S(1)}, u32[]{:S(2)}, u32[]{:S(2)}) collective-permute-start(bf16[104,512]{1,0:T(8,128)(2,1)S(1)} %get-tuple-element.98), channel_id=1, source_target_pairs={{0,24},{1,25},{2,26},{3,27},{4,28},{5,29},{6,30},{7,31},{8,16},{9,... | collective-permute-start | bytes 319496 | tf_op jit(solution)/shard_map/ppermute | solution.py:181
  145.7 24.1 %collective-permute-start.18 = (bf16[104,512]{1,0:T(8,128)(2,1)S(1)}, bf16[104,512]{1,0:T(8,128)(2,1)S(1)}, u32[]{:S(2)}, u32[]{:S(2)}) collective-permute-start(bf16[104,512]{1,0:T(8,128)(2,1)S(1)} %get-tuple-element.97), channel_id=1, source_target_pairs={{0,16},{1,17},{2,18},{3,19},{4,20},{5,21},{6,22},{7,23},{8,24},{9,... | collective-permute-start | bytes 319496 | tf_op jit(solution)/shard_map/ppermute | solution.py:181
  147.5 22.3 %collective-permute-start.14 = (bf16[104,512]{1,0:T(8,128)(2,1)S(1)}, bf16[104,512]{1,0:T(8,128)(2,1)S(1)}, u32[]{:S(2)}, u32[]{:S(2)}) collective-permute-start(bf16[104,512]{1,0:T(8,128)(2,1)S(1)} %get-tuple-element.96), channel_id=1, source_target_pairs={{0,8},{1,9},{2,10},{3,11},{4,12},{5,13},{6,14},{7,15},{8,0},{9,1},... | collective-permute-start | bytes 319496 | tf_op jit(solution)/shard_map/ppermute | solution.py:181
  149.1 3.2 %copy-start.13 = (bf16[2048,512]{1,0:T(8,128)(2,1)S(1)}, bf16[2048,512]{1,0:T(8,128)(2,1)}, u32[]{:S(2)}) copy-start(bf16[2048,512]{1,0:T(8,128)(2,1)} %convolution_convert_fusion.1) | copy-start | bytes 6291460
  165.8 7.6 %copy-start.1 = (bf16[1,2048,512]{2,1,0:T(8,128)(2,1)S(1)}, bf16[1,2048,512]{2,1,0:T(8,128)(2,1)}, u32[]{:S(2)}) copy-start(bf16[1,2048,512]{2,1,0:T(8,128)(2,1)} %param.12) | copy-start | bytes 6291460

commit v2 on v0

--- a/solution.py
+++ b/solution.py
@@ -1,6 +1,8 @@
 import jax
 import jax.numpy as jnp
 from jax import lax
+from jax.experimental import pallas as pl
+from jax.experimental.pallas import tpu as pltpu
 from jax.sharding import PartitionSpec as P
 
 BLOCKS = 2
@@ -158,6 +160,356 @@
     )
     return (token_grad, gate_grad, grad_gate[None], grad_up[None], grad_down[None], router_grad)
 
+def dot_of(a, b, ca, cb):
+    return lax.dot_general(a, b, (((ca,), (cb,)), ((), ())), preferred_element_type=jnp.float32)
+
+
+def as_column(row):
+    n = row.shape[1]
+    same = lax.broadcasted_iota(jnp.int32, (n, n), 0) == lax.broadcasted_iota(jnp.int32, (n, n), 1)
+    return jnp.sum(jnp.where(same, row, 0.0), axis=1, keepdims=True)
+
+
+def as_row(column):
+    n = column.shape[0]
+    same = lax.broadcasted_iota(jnp.int32, (n, n), 0) == lax.broadcasted_iota(jnp.int32, (n, n), 1)
+    return jnp.sum(jnp.where(same, column, 0.0), axis=0, keepdims=True)
+
+
+def fast_shards(tokens, cotangent, routes, router, w_gate, w_up, w_down):
+    f32, bf16, i32 = jnp.float32, jnp.bfloat16, jnp.int32
+    axes = ("ep", "tp")
+    ep_count = lax.axis_size("ep")
+    tp_count = lax.axis_size("tp")
+    total = ep_count * tp_count
+    experts = ep_count // BLOCKS
+    rows, width = tokens.shape
+    top = routes.shape[1]
+    cap = 3 * rows * top // (2 * experts)
+    quarter = width // tp_count
+    hid = w_gate.shape[2]
+    chunk = width // total
+    pad = -(-(1 + experts) // 8) * 8
+    tall = cap + pad
+    vmem = pl.BlockSpec(memory_space=pltpu.VMEM)
+    anywhere = pl.BlockSpec(memory_space=pl.ANY)
+
+    def near_memory(values):
+        return [pltpu.with_memory_space_constraint(v, pltpu.VMEM) for v in values]
+
+    def call(body, name, args, outs, flops, mib, scratch=(), far=0):
+        near = len(outs) - far
+        return pl.pallas_call(
+            body,
+            out_shape=[pltpu.VMEM(*o) for o in outs[:near]] + [jax.ShapeDtypeStruct(*o) for o in outs[near:]],
+            in_specs=[vmem] * len(args),
+            out_specs=[vmem] * near + [anywhere] * far,
+            scratch_shapes=list(scratch),
+            compiler_params=pltpu.CompilerParams(vmem_limit_bytes=mib << 20),
+            cost_estimate=pl.CostEstimate(flops=int(flops), bytes_accessed=1 << 20, transcendentals=0),
+            name=name,
+        )(*near_memory(args))
+
+    def swap(value, bits):
+        return lax.ppermute(value, axes, [(i, i ^ bits) for i in range(total)])
+
+    def mixed(value, bits_even, bits_odd):
+        return lax.ppermute(
+            value, axes, [(i, i ^ (bits_odd if i % 2 else bits_even)) for i in range(total)]
+        )
+
+    cbit, ybit, xbit, zbit = 1, 2, tp_count, tp_count * BLOCKS
+
+    def pack_body(tok_ref, cot_ref, route_ref, router_ref, *outs):
+        packed, place_ref, product_ref, first_ref = outs[:experts], outs[experts], outs[experts + 1], outs[experts + 2]
+        tp = lax.axis_index("tp")
+        here = lax.axis_index("ep") // BLOCKS
+        logits = dot_of(tok_ref[...], router_ref[...], 1, 1)
+        r0 = as_column(route_ref[0:1, :].astype(f32)).astype(i32)
+        r1 = as_column(route_ref[1:2, :].astype(f32)).astype(i32)
+        lane = lax.broadcasted_iota(i32, (rows, experts), 1)
+        c0 = jnp.sum(jnp.where(lane == r0, logits, 0.0), axis=1, keepdims=True)
+        c1 = jnp.sum(jnp.where(lane == r1, logits, 0.0), axis=1, keepdims=True)
+        w0, w1 = jax.nn.sigmoid(c0 - c1), jax.nn.sigmoid(c1 - c0)
+        product = w0 * w1
+        product_ref[...] = jnp.broadcast_to(product, product_ref.shape)
+        wide = lax.broadcasted_iota(i32, first_ref.shape, 1)
+        first_ref[...] = jnp.where(wide == 0, r0, r1)
+        near = here ^ lane
+        hit = (near == r0) | (near == r1)
+        below = lax.broadcasted_iota(i32, (rows, rows), 1) <= lax.broadcasted_iota(i32, (rows, rows), 0)
+        rank = dot_of(below.astype(bf16), hit.astype(bf16), 1, 0)
+        rank = jnp.where(hit, rank - 1.0, -1.0)
+        slot = lax.broadcasted_iota(i32, (rows, rows), 1).astype(f32)
+        kind = lax.broadcasted_iota(i32, (rows, 128), 1)
+        hi = product.astype(bf16).astype(f32)
+        lo = product - hi
+        spot = pl.multiple_of(tp * quarter, quarter)
+        tok = tok_ref[:, pl.ds(spot, quarter)]
+        cot = cot_ref[:, pl.ds(spot, quarter)]
+        for j in range(experts):
+            place = (rank[:, j : j + 1] == slot).astype(f32).astype(bf16)
+            place_ref[:, j * rows : (j + 1) * rows] = place
+            first = r0 == (here ^ j)
+            gate = jnp.where(first, w0, w1)
+            other = jnp.where(first, r1, r0).astype(f32)
+            meta = jnp.where(
+                kind == 0, gate, jnp.where(kind == 1, hi, jnp.where(kind == 2, lo, jnp.where(kind == 3, other, 0.0)))
+            ).astype(bf16)
+            packed[j][0:cap, 0:quarter] = dot_of(place, tok, 0, 0)[0:cap].astype(bf16)
+            packed[j][0:cap, quarter:] = dot_of(place, cot, 0, 0)[0:cap].astype(bf16)
+            packed[j][cap:, :] = jnp.zeros((pad, 2 * quarter), bf16)
+            packed[j][cap : cap + 8, 0:rows] = dot_of(meta, place, 0, 0)[0:8].astype(bf16)
+
+    outs = call(
+        pack_body,
+        "pack",
+        (tokens, cotangent, routes.T, router.T),
+        [((tall, 2 * quarter), bf16)] * experts + [((rows, experts * rows), bf16), ((rows, 128), f32), ((rows, 128), i32)],
+        4 * rows * rows * quarter * experts,
+        24,
+    )
+    packed, place, product, named = outs[:experts], outs[experts], outs[experts + 1], outs[experts + 2]
+
+    half = experts // 2
+    pieces = [list(range(half)), list(range(half, experts))]
+    slots = quarter // (2 * chunk)
+
+    def order(blocks):
+        own, side, over, diag, town, tside, tover, tdiag = blocks
+        return [[own, side], [town, tside], [over, diag], [tover, tdiag]]
+
+    def rows_of(pair, kp, base):
+        return jnp.concatenate(
+            [ref[n, 0:cap, base : base + quarter] for ref in pair for n in range(kp)], axis=0
+        )
+
+    def gates_of(own, side, kp, kind):
+        return jnp.concatenate(
+            [as_column(ref[n, cap + kind : cap + kind + 1, 0:cap].astype(f32)) for ref in (own, side) for n in range(kp)],
+            axis=0,
+        )
+
+    def forward(blocks, kp, weights):
+        n = BLOCKS * kp * cap
+
+        def body(*refs):
+            quarters = order(refs[:8])
+            wg_ref, wu_ref, wd_ref, x_ref, s_ref, hid_ref, dg_ref, du_ref, term_ref, sum_ref, c_ref = refs[8:]
+            tp = lax.axis_index("tp")
+            here = lax.axis_index("ep") // BLOCKS
+            gate = gates_of(refs[0], refs[1], kp, 0)
+            for r in range(tp_count):
+                spot = pl.multiple_of((tp ^ r) * quarter, quarter)
+                x_ref[:, pl.ds(spot, quarter)] = rows_of(quarters[r], kp, 0)
+                cot = rows_of(quarters[r], kp, quarter)
+                c_ref[:, pl.ds(spot, quarter)] = cot
+                s_ref[:, pl.ds(spot, quarter)] = (gate * cot.astype(f32)).astype(bf16)
+            term = jnp.zeros((n, 1), f32)
+            for h in range(2):
+                cols = slice(h * hblock, (h + 1) * hblock)
+                pre_gate = dot_of(x_ref[...], wg_ref[:, cols], 1, 0)
+                pre_up = dot_of(x_ref[...], wu_ref[:, cols], 1, 0)
+                back = dot_of(c_ref[...], wd_ref[cols, :], 1, 1)
+                sig = jax.nn.sigmoid(pre_gate)
+                active = pre_gate * sig
+                hidden = (active * pre_up).astype(bf16)
+                hid_ref[:, cols] = hidden
+                term += jnp.sum(hidden.astype(f32) * back, axis=1, keepdims=True)
+                scaled = gate * back
+                dg_ref[:, cols] = (scaled * pre_up * sig * (1.0 + pre_gate * (1.0 - sig))).astype(bf16)
+                du_ref[:, cols] = (scaled * active).astype(bf16)
+            term_ref[...] = jnp.broadcast_to(term, (n, 128))
+            prod = gates_of(refs[0], refs[1], kp, 1) + gates_of(refs[0], refs[1], kp, 2)
+            other = gates_of(refs[0], refs[1], kp, 3)
+            lane = lax.broadcasted_iota(i32, (n, 128), 1)
+            name = (lane % pad - 1).astype(f32)
+            sign = jnp.where(name == here.astype(f32), 1.0, 0.0) - jnp.where(name == other, 1.0, 0.0)
+            full = jnp.where(lane < 2 * pad, (prod * term) * sign, 0.0)
+            upper = full.astype(bf16)
+            lower = (full - upper.astype(f32)).astype(bf16)
+            got = dot_of(jnp.where(lane < pad, upper, lower), x_ref[...], 0, 0)
+            sum_ref[...] = got[0:pad] + got[pad : 2 * pad]
+
+        return call(
+            body,
+            "forward",
+            (*blocks, *weights),
+            [((n, width), bf16)] * 2 + [((n, hid), bf16)] * 3 + [((n, 128), f32), ((pad, width), f32)],
+            6 * n * width * hid,
+            24,
+            [pltpu.VMEM((n, width), bf16)],
+        )
+
+    def input_grads(d_gate, d_up, terms, sums, weights, piece, flip):
+        kp = len(piece)
+        final = piece is pieces[-1]
+        others = [j for j in range(experts) if j not in piece]
+
+        def body(*refs):
+            dg_ref, du_ref, term_ref, wg_ref, wu_ref = refs[:5]
+            sum_refs, out_ref = refs[5:-1], refs[-1]
+            ep, tp = lax.axis_index("ep"), lax.axis_index("tp")
+            core = (tp % 2) ^ flip
+            term = term_ref[:, 0:1]
+            top_row = lax.broadcasted_iota(i32, (pad, 128), 0) == 0
+            for dy in range(2):
+                r = 2 * dy + flip
+                spot = pl.multiple_of((tp ^ r) * quarter, quarter)
+                dx = dot_of(dg_ref[...], wg_ref[pl.ds(spot, quarter), :], 1, 1)
+                dx += dot_of(du_ref[...], wu_ref[pl.ds(spot, quarter), :], 1, 1)
+                dx = dx.astype(bf16)
+                for b in range(BLOCKS):
+                    k = jnp.where(core == 0, 2 * dy + b, 2 * b + dy)
+
+                    def total_of(j):
+                        target = (ep * tp_count + tp) ^ ((j * BLOCKS + b) * tp_count + r)
+                        at = pl.multiple_of((target // 2) * (2 * chunk), 2 * chunk)
+                        found = sum_refs[0][:, pl.ds(at, 2 * chunk)]
+                        for ref in sum_refs[1:]:
+                            found += ref[:, pl.ds(at, 2 * chunk)]
+                        return found
+
+                    for m, j in enumerate(piece):
+                        g = (b * kp + m) * cap
+                        out_ref[k, m, 0:cap, :] = dx[g : g + cap]
+                        extra = jnp.pad(as_row(term[g : g + cap]), ((0, 0), (0, 128 - cap)))
+                        extra = jnp.where(top_row, extra, total_of(j) if final else 0.0)
+                        out_ref[k, m, cap:, :] = jnp.zeros((pad, quarter), bf16)
+                        out_ref[k, m, cap:, 0 : 2 * chunk] = extra.astype(bf16)
+                        if final:
+                            for s, o in enumerate(others[m::kp]):
+                                lanes = slice((s + 1) * 2 * chunk, (s + 2) * 2 * chunk)
+                                out_ref[k, m, cap:, lanes] = total_of(o).astype(bf16)
+
+        return call(
+            body,
+            "input_grads",
+            (d_gate, d_up, terms, *weights[:2], *(sums if final else ())),
+            [((4, kp, tall, quarter), bf16)],
+            2 * BLOCKS * kp * cap * width * hid,
+            16,
+        )[0]
+
+    hblock = hid // 2
+    weights = (w_gate[0], w_up[0], w_down[0])
+    kept, backs, sums, router_parts = [], [None] * experts, [], []
+    for piece in pieces:
+        kp = len(piece)
+        own = jnp.stack([packed[j] if j == 0 else swap(packed[j], zbit * j) for j in piece])
+        side = swap(own, xbit)
+        over = swap(own, ybit)
+        core = lax.axis_index("tp") % 2
+        diag = mixed(jnp.where(core == 0, side, over), ybit, xbit)
+        blocks = [own, side, over, diag] + [swap(v, cbit) for v in (own, side, over, diag)]
+        x_in, s_cot, hidden, d_gate, d_up, terms, part = forward(blocks, kp, weights)
+        sums.append(part)
+        send = input_grads(d_gate, d_up, terms, sums, weights, piece, 1)
+        gained = swap(send, cbit)
+        keep = input_grads(d_gate, d_up, terms, sums, weights, piece, 0)
+        summed = keep.astype(f32) + gained.astype(f32)
+        first = mixed(summed[2:].astype(bf16), ybit, xbit)
+        both = summed[:2] + first.astype(f32)
+        last = both[0] + mixed(both[1].astype(bf16), xbit, ybit).astype(f32)
+        last = last.astype(bf16)
+        for m, j in enumerate(piece):
+            backs[j] = last[m] if j == 0 else swap(last[m], zbit * j)
+        if piece is pieces[-1]:
+            others = [j for j in range(experts) if j not in piece]
+            for m in range(kp):
+                for s, o in enumerate(others[m::kp]):
+                    value = last[m, cap:, (s + 1) * 2 * chunk : (s + 2) * 2 * chunk]
+                    router_parts.append(value if o == 0 else swap(value, zbit * o))
+        kept.append((x_in, s_cot, hidden, d_gate, d_up))
+
+    def weight_body(*refs):
+        acts = [refs[5 * p : 5 * p + 5] for p in range(len(pieces))]
+        outs, bufs, sems = refs[-7:-4], refs[-4:-1], refs[-1]
+        hidden, d_gate, d_up = (jnp.concatenate([a[i][...] for a in acts], axis=0) for i in range(2, 5))
+        copies = []
+        for r in range(tp_count):
+            cols = slice(r * quarter, (r + 1) * quarter)
+            tok = jnp.concatenate([a[0][:, cols] for a in acts], axis=0)
+            cot = jnp.concatenate([a[1][:, cols] for a in acts], axis=0)
+            bufs[0][cols, :] = dot_of(tok, d_gate, 0, 0).astype(bf16)
+            bufs[1][cols, :] = dot_of(tok, d_up, 0, 0).astype(bf16)
+            bufs[2][:, cols] = dot_of(hidden, cot, 0, 0).astype(bf16)
+            for i in range(3):
+                where = (cols, slice(None)) if i < 2 else (slice(None), cols)
+                copy = pltpu.make_async_copy(bufs[i].at[where], outs[i].at[where], sems.at[3 * r + i])
+                copy.start()
+                copies.append(copy)
+        for copy in copies:
+            copy.wait()
+
+    grad_gate, grad_up, grad_down = call(
+        weight_body,
+        "weight_grads",
+        [v for k in kept for v in k],
+        [((width, hid), bf16), ((width, hid), bf16), ((hid, width), bf16)],
+        6 * BLOCKS * experts * cap * width * hid,
+        40,
+        [
+            pltpu.VMEM((width, hid), bf16),
+            pltpu.VMEM((width, hid), bf16),
+            pltpu.VMEM((hid, width), bf16),
+            pltpu.SemaphoreType.DMA((3 * tp_count,)),
+        ],
+        far=3,
+    )
+
+    def finish_body(*refs):
+        back, parts = refs[:experts], refs[experts : experts + len(router_parts)]
+        place_ref, product_ref, named_ref, router_ref, tok_out, gate_out, router_out = refs[experts + len(router_parts) :]
+        tp = lax.axis_index("tp")
+        here = lax.axis_index("ep") // BLOCKS
+        r0, r1 = named_ref[:, 0:1], named_ref[:, 1:2]
+        routed = jnp.zeros((rows, quarter), f32)
+        g0 = jnp.zeros((rows, 1), f32)
+        g1 = jnp.zeros((rows, 1), f32)
+        sums = jnp.zeros((pad, 2 * chunk), f32)
+        for j in range(experts):
+            place = place_ref[:, j * rows : j * rows + cap]
+            routed += dot_of(place, back[j][0:cap, :], 1, 0)
+            per = jnp.sum(place.astype(f32) * back[j][cap : cap + 1, 0:cap].astype(f32), axis=1, keepdims=True)
+            g0 += jnp.where(r0 == (here ^ j), per, 0.0)
+            g1 += jnp.where(r1 == (here ^ j), per, 0.0)
+            if j in pieces[-1]:
+                sums += back[j][cap:, 0 : 2 * chunk].astype(f32)
+        for part in parts:
+            sums += part[...].astype(f32)
+        lane2 = lax.broadcasted_iota(i32, (rows, top), 1)
+        gate_out[...] = jnp.where(lane2 == 0, g0, g1)
+        lead = product_ref[:, 0:1] * (g0 - g1)
+        lane = lax.broadcasted_iota(i32, (rows, experts), 1)
+        lgrad = jnp.where(lane == r0, lead, 0.0) - jnp.where(lane == r1, lead, 0.0)
+        upper = lgrad.astype(bf16)
+        lower = (lgrad - upper.astype(f32)).astype(bf16)
+        cols = router_ref[:, pl.ds(pl.multiple_of(tp * quarter, quarter), quarter)]
+        routed += dot_of(upper, cols, 1, 0) + dot_of(lower, cols, 1, 0)
+        tok_out[...] = routed.astype(bf16)
+        router_out[...] = jnp.where(tp % 2 == 0, sums[1 : 1 + experts, 0:chunk], sums[1 : 1 + experts, chunk : 2 * chunk])
+
+    args = (*backs, *router_parts, place, product, named, router.T)
+    token_grad, gate_grad, router_sum = pl.pallas_call(
+        finish_body,
+        out_shape=[
+            jax.ShapeDtypeStruct((rows, quarter), bf16),
+            jax.ShapeDtypeStruct((rows, top), f32),
+            jax.ShapeDtypeStruct((experts, chunk), f32),
+        ],
+        in_specs=[vmem] * len(args),
+        out_specs=[vmem] * 3,
+        compiler_params=pltpu.CompilerParams(vmem_limit_bytes=16 << 20),
+        name="finish",
+    )(*near_memory(args))
+    return (token_grad, gate_grad, grad_gate[None], grad_up[None], grad_down[None], router_sum.T)
+
+
+def fits(mesh):
+    experts = mesh.shape["ep"] // BLOCKS
+    return mesh.shape["tp"] == 4 and experts * BLOCKS == mesh.shape["ep"] and experts & (experts - 1) == 0
+
 
 def solution(mesh):
     placed = (
@@ -170,7 +522,7 @@
         P("ep", "tp", None),
     )
     return jax.shard_map(
-        shards,
+        fast_shards if fits(mesh) else shards,
         mesh=mesh,
         in_specs=placed,
         out_specs=(

time: 326 us -> 101 us (0.31)
  waiting for transfers between devices: 185 us -> 42.3 us
  blocking collectives: 65.4 us -> 0 us
  matrix products: 39.1 us -> 0 us
  Pallas kernels: 0 us -> 22 us
  starting transfers between devices: 11.3 us -> 25.4 us
  between operations: 14 us -> 1 us
    unnamed x5 -> x0, waiting for transfers between devices: 122 us -> none
    all_to_all x3 -> x0, blocking collectives: 59.5 us -> none  [the longest x1 27.3 us: shards(): lax.all_to_all(pack_rows(tok_part), 'ep', split_axis=0, concat_axis=0, ti...]
    ppermute x0 -> x27, waiting for transfers between devices: none -> 42.3 us  [the longest x21 22.7 us: swap(): return lax.ppermute(value, axes, [(i, i ^ bits) for i in range(total)])]
    dot_general x15 -> x0, matrix products: 37.3 us -> none  [the longest x1 6.74 us: expert_grads(): lax.dot_general(cot_in, down_weight, (((1,), (1,)), ((), ())), preferred_...]
    reduce_scatter x1 -> x0, waiting for transfers between devices: 33.2 us -> none  [shards(): lax.psum_scatter(partial_dx.reshape(ep_count, capacity, width).astype(jnp...]
    ppermute x0 -> x27, starting transfers between devices: none -> 25.4 us  [the longest x21 18.2 us: swap(): return lax.ppermute(value, axes, [(i, i ^ bits) for i in range(total)])]
    all_gather x2 -> x0, waiting for transfers between devices: 23.9 us -> none  [the longest x1 21.4 us: shards(): lax.all_gather(recv_cot_part, 'tp', axis=2, tiled=True)]
    pallas_call x0 -> x9, Pallas kernels: none -> 22 us  [the longest x8 20.8 us: call(): pl.pallas_call(body, out_shape=[pltpu.VMEM(*o) for o in outs[:near]] + [j...]
  transfers between devices with their start and end apart: 6 -> 27, of which waited for: 5 -> 9; matrix products, arithmetic and copies ran while one was open for 8% -> 3% of each run, Pallas kernels for 0% -> 15%
where the time goes in v2:
time: 101 us
  waiting for transfers between devices  42.3 us (42%)
  starting transfers between devices  25.4 us (25%)
  Pallas kernels  22 us (22%)
  local copies, waits for them, and re-layouts  7.52 us (7%)
  other arithmetic  2.84 us (3%)
    ppermute x21, waiting for transfers between devices, swap(): return lax.ppermute(value, axes, [(i, i ^ bits) for i in range(total)])  22.7 us
    pallas_call x8, Pallas kernels, call(): pl.pallas_call(body, out_shape=[pltpu.VMEM(*o) for o in outs[:near]] + [j...  20.8 us
    ppermute x6, waiting for transfers between devices, mixed(): lax.ppermute(value, axes, [(i, i ^ (bits_odd if i % 2 else bits_even)) fo...  19.6 us
    ppermute x21, starting transfers between devices, swap(): return lax.ppermute(value, axes, [(i, i ^ bits) for i in range(total)])  18.2 us
    unnamed x29, local copies, waits for them, and re-layouts  7.32 us
    ppermute x6, starting transfers between devices, mixed(): lax.ppermute(value, axes, [(i, i ^ (bits_odd if i % 2 else bits_even)) fo...  7.19 us
  transfers between devices with their start and end apart: 27, of which 9 were waited for; matrix products, arithmetic and copies ran while one was open for 3% of the time, Pallas kernels for 15%

profile of v2, /device:TPU:0, one launch (start us, length us, event | category | flops | bytes accessed | tf_op | source)
XLA Modules:
  0.0 101.0 jit_solution(17673306367689159981)
XLA Ops:
  0.6 1.0 %copy-done.5 = bf16[128,2048]{1,0:T(8,128)(2,1)S(1)} copy-done((bf16[128,2048]{1,0:T(8,128)(2,1)S(1)}, bf16[128,2048]{1,0:T(8,128)(2,1)}, u32[]{:S(2)}) %copy-start.5) | copy-done | bytes 524312
  1.7 1.0 %copy-done.6 = bf16[128,2048]{1,0:T(8,128)(2,1)S(1)} copy-done((bf16[128,2048]{1,0:T(8,128)(2,1)S(1)}, bf16[128,2048]{1,0:T(8,128)(2,1)}, u32[]{:S(2)}) %copy-start.6) | copy-done | bytes 524312
  2.7 0.7 copy-done.7
  3.4 0.7 copy-done.13
  4.1 1.0 pack.1
  5.1 3.1 %collective-permute-start = (bf16[104,1024]{1,0:T(8,128)(2,1)S(1)}, bf16[104,1024]{1,0:T(8,128)(2,1)S(1)}, u32[]{:S(2)}, u32[]{:S(2)}) collective-permute-start(bf16[104,1024]{1,0:T(8,128)(2,1)S(1)} %get-tuple-element.34), channel_id=1, source_target_pairs={{0,8},{1,9},{2,10},{3,11},{4,12},{5,13},{6,14},{7,15},{8,0},{9,1},... | collective-permute-start | bytes 638984 | tf_op jit(solution)/shard_map/ppermute | solution.py:214
  8.3 2.5 %collective-permute-start.13 = (bf16[104,1024]{1,0:T(8,128)(2,1)S(1)}, bf16[104,1024]{1,0:T(8,128)(2,1)S(1)}, u32[]{:S(2)}, u32[]{:S(2)}) collective-permute-start(bf16[104,1024]{1,0:T(8,128)(2,1)S(1)} %get-tuple-element.39), channel_id=1, source_target_pairs={{0,24},{1,25},{2,26},{3,27},{4,28},{5,29},{6,30},{7,31},{8,16},{9,... | collective-permute-start | bytes 638984 | tf_op jit(solution)/shard_map/ppermute | solution.py:214
  10.9 3.0 %collective-permute-done = bf16[104,1024]{1,0:T(8,128)(2,1)S(1)} collective-permute-done((bf16[104,1024]{1,0:T(8,128)(2,1)S(1)}, bf16[104,1024]{1,0:T(8,128)(2,1)S(1)}, u32[]{:S(2)}, u32[]{:S(2)}) %collective-permute-start) | collective-permute-done | bytes 213024 | tf_op jit(solution)/shard_map/ppermute | solution.py:214
  13.9 0.8 pad_maximum_fusion.refs_0_
  14.7 1.5 %collective-permute-start.1 = (bf16[2,104,1024]{2,1,0:T(8,128)(2,1)}, bf16[2,104,1024]{2,1,0:T(8,128)(2,1)}, u32[]{:S(2)}, u32[]{:S(2)}) collective-permute-start(bf16[2,104,1024]{2,1,0:T(8,128)(2,1)} %pad_maximum_fusion.refs_0_), channel_id=1, source_target_pairs={{0,4},{1,5},{2,6},{3,7},{4,0},{5,1},{6,2},{7,3},{8,12},{9,13},{10,... | collective-permute-start | bytes 1277960 | tf_op jit(solution)/shard_map/ppermute | solution.py:214
  16.2 1.5 %collective-permute-start.2 = (bf16[2,104,1024]{2,1,0:T(8,128)(2,1)}, bf16[2,104,1024]{2,1,0:T(8,128)(2,1)}, u32[]{:S(2)}, u32[]{:S(2)}) collective-permute-start(bf16[2,104,1024]{2,1,0:T(8,128)(2,1)} %pad_maximum_fusion.refs_0_), channel_id=1, source_target_pairs={{0,2},{1,3},{2,0},{3,1},{4,6},{5,7},{6,4},{7,5},{8,10},{9,11},{10,... | collective-permute-start | bytes 1277960 | tf_op jit(solution)/shard_map/ppermute | solution.py:214
  17.7 3.8 %collective-permute-done.13 = bf16[104,1024]{1,0:T(8,128)(2,1)S(1)} collective-permute-done((bf16[104,1024]{1,0:T(8,128)(2,1)S(1)}, bf16[104,1024]{1,0:T(8,128)(2,1)S(1)}, u32[]{:S(2)}, u32[]{:S(2)}) %collective-permute-start.13) | collective-permute-done | bytes 213024 | tf_op jit(solution)/shard_map/ppermute | solution.py:214
  21.5 8.0 %collective-permute-done.12 = bf16[104,1024]{1,0:T(8,128)(2,1)S(1)} collective-permute-done((bf16[104,1024]{1,0:T(8,128)(2,1)S(1)}, bf16[104,1024]{1,0:T(8,128)(2,1)S(1)}, u32[]{:S(2)}, u32[]{:S(2)}) %collective-permute-start.12) | collective-permute-done | bytes 213024 | tf_op jit(solution)/shard_map/ppermute | solution.py:214
  29.6 1.6 %collective-permute-start.14 = (bf16[2,104,1024]{2,1,0:T(8,128)(2,1)S(1)}, bf16[2,104,1024]{2,1,0:T(8,128)(2,1)S(1)}, u32[]{:S(2)}, u32[]{:S(2)}) collective-permute-start(bf16[2,104,1024]{2,1,0:T(8,128)(2,1)S(1)} %pad_maximum_fusion.1.refs_0_), channel_id=1, source_target_pairs={{0,4},{1,5},{2,6},{3,7},{4,0},{5,1},{6,2},{7,3},{8,12},{9,13},{10,... | collective-permute-start | bytes 1277960 | tf_op jit(solution)/shard_map/ppermute | solution.py:214
  31.1 1.5 %collective-permute-start.15 = (bf16[2,104,1024]{2,1,0:T(8,128)(2,1)S(1)}, bf16[2,104,1024]{2,1,0:T(8,128)(2,1)S(1)}, u32[]{:S(2)}, u32[]{:S(2)}) collective-permute-start(bf16[2,104,1024]{2,1,0:T(8,128)(2,1)S(1)} %pad_maximum_fusion.1.refs_0_), channel_id=1, source_target_pairs={{0,2},{1,3},{2,0},{3,1},{4,6},{5,7},{6,4},{7,5},{8,10},{9,11},{10,... | collective-permute-start | bytes 1277960 | tf_op jit(solution)/shard_map/ppermute | solution.py:214
  32.7 1.1 %broadcast_select_fusion.1 = bf16[2,104,1024]{2,1,0:T(8,128)(2,1)S(1)} fusion(bf16[2,104,1024]{2,1,0:T(8,128)(2,1)} %collective-permute-done.1.refs_1_, bf16[2,104,1024]{2,1,0:T(8,128)(2,1)} %collective-permute-done.2.refs_2_, pred[]{:T(512)S(6)} %eq.7), kind=kLoop, calls=%fused_computation.17 | loop fusion | flops 212992 | bytes 1277953 | tf_op jit(solution)/shard_map/jit(_where)/select_n | solution.py:403
  33.7 0.6 collective-permute-start.3
  34.3 0.2 collective-permute-start.5
  34.5 7.8 %collective-permute-done.14.refs_1_ = bf16[2,104,1024]{2,1,0:T(8,128)(2,1)S(1)} collective-permute-done((bf16[2,104,1024]{2,1,0:T(8,128)(2,1)S(1)}, bf16[2,104,1024]{2,1,0:T(8,128)(2,1)S(1)}, u32[]{:S(2)}, u32[]{:S(2)}) %collective-permute-start.14) | collective-permute-done | bytes 426016 | tf_op jit(solution)/shard_map/ppermute | solution.py:214
  42.4 1.6 %collective-permute-start.16 = (bf16[2,104,1024]{2,1,0:T(8,128)(2,1)S(1)}, bf16[2,104,1024]{2,1,0:T(8,128)(2,1)S(1)}, u32[]{:S(2)}, u32[]{:S(2)}) collective-permute-start(bf16[2,104,1024]{2,1,0:T(8,128)(2,1)S(1)} %broadcast_select_fusion), channel_id=1, source_target_pairs={{0,2},{1,5},{2,0},{3,7},{4,6},{5,1},{6,4},{7,3},{8,10},{9,13},{10,... | collective-permute-start | bytes 1277960 | tf_op jit(solution)/shard_map/ppermute | solution.py:217
  44.0 2.1 %collective-permute-done.3.refs_3_ = bf16[2,104,1024]{2,1,0:T(8,128)(2,1)S(1)} collective-permute-done((bf16[2,104,1024]{2,1,0:T(8,128)(2,1)S(1)}, bf16[2,104,1024]{2,1,0:T(8,128)(2,1)S(1)}, u32[]{:S(2)}, u32[]{:S(2)}) %collective-permute-start.3) | collective-permute-done | bytes 426016 | tf_op jit(solution)/shard_map/ppermute | solution.py:217
  46.1 0.5 collective-permute-start.17
  46.7 0.4 collective-permute-start.19
  47.1 3.5 %collective-permute-done.16.refs_3_ = bf16[2,104,1024]{2,1,0:T(8,128)(2,1)S(1)} collective-permute-done((bf16[2,104,1024]{2,1,0:T(8,128)(2,1)S(1)}, bf16[2,104,1024]{2,1,0:T(8,128)(2,1)S(1)}, u32[]{:S(2)}, u32[]{:S(2)}) %collective-permute-start.16) | collective-permute-done | bytes 426016 | tf_op jit(solution)/shard_map/ppermute | solution.py:217
  50.7 1.6 %copy-done.1 = bf16[1,2048,512]{2,1,0:T(8,128)(2,1)S(1)} copy-done((bf16[1,2048,512]{2,1,0:T(8,128)(2,1)S(1)}, bf16[1,2048,512]{2,1,0:T(8,128)(2,1)}, u32[]{:S(2)}) %copy-start.1) | copy-done | bytes 2097176
  52.3 1.6 %copy-done.3 = bf16[1,512,2048]{2,1,0:T(8,128)(2,1)S(1)} copy-done((bf16[1,512,2048]{2,1,0:T(8,128)(2,1)S(1)}, bf16[1,512,2048]{2,1,0:T(8,128)(2,1)}, u32[]{:S(2)}) %copy-start.3) | copy-done | bytes 2097176
  53.9 5.5 %forward.2 = (bf16[384,2048]{1,0:T(8,128)(2,1)S(1)}, bf16[384,2048]{1,0:T(8,128)(2,1)S(1)}, bf16[384,512]{1,0:T(8,128)(2,1)S(1)}, bf16[384,512]{1,0:T(8,128)(2,1...) custom-call(bf16[2,104,1024]{2,1,0:T(8,128)(2,1)} %pad_maximum_fusion.refs_0_, ...), custom_call_target="tpu_custom_call" | custom-call | flops 2415919104 | bytes 1048576 | tf_op jit(solution)/shard_map/forward/pallas_call | solution.py:202
  59.4 4.1 %forward.3 = (bf16[384,2048]{1,0:T(8,128)(2,1)S(1)}, bf16[384,2048]{1,0:T(8,128)(2,1)S(1)}, bf16[384,512]{1,0:T(8,128)(2,1)S(1)}, bf16[384,512]{1,0:T(8,128)(2,1...) custom-call(bf16[2,104,1024]{2,1,0:T(8,128)(2,1)S(1)} %pad_maximum_fusion.1.refs_0_, ...), custom_call_target="tpu_custom_call" | custom-call | flops 2415919104 | bytes 1048576 | tf_op jit(solution)/shard_map/forward/pallas_call | solution.py:202
  63.5 1.0 %input_grads.7 = bf16[4,2,104,512]{3,2,1,0:T(8,128)(2,1)S(1)} custom-call(bf16[384,512]{1,0:T(8,128)(2,1)S(1)} %get-tuple-element.40.refs_0_.refs_8_, bf16[384,512]{1,0:T(8,128)(2,1)S(1)} %get-tuple-element.41.refs_1_.refs_9_, f32[384,128]{1,0:T(8,128)S(1)} %get-tuple-element.42.refs_2_, bf16[2048,512]{1,0:T(8,128)(2,1)S(1)} %bitcast.43, ...), custom_call_target="tpu_custom_call" | custom-call | flops 805306368 | bytes 1048576 | tf_op jit(solution)/shard_map/input_grads/pallas_call | solution.py:202
  64.5 0.6 collective-permute-start.21
  65.1 1.0 input_grads.5
  66.2 1.0 input_grads.6
  67.2 0.3 convert_add_fusion
  67.5 1.6 %collective-permute-start.22 = (bf16[2,2,104,512]{3,2,1,0:T(8,128)(2,1)S(1)}, bf16[2,2,104,512]{3,2,1,0:T(8,128)(2,1)S(1)}, u32[]{:S(2)}, u32[]{:S(2)}) collective-permute-start(bf16[2,2,104,512]{3,2,1,0:T(8,128)(2,1)S(1)} %slice.100), channel_id=1, source_target_pairs={{0,2},{1,5},{2,0},{3,7},{4,6},{5,1},{6,4},{7,3},{8,10},{9,13},{10,... | collective-permute-start | bytes 1277960 | tf_op jit(solution)/shard_map/ppermute | solution.py:217
  69.1 1.2 %input_grads.4 = bf16[4,2,104,512]{3,2,1,0:T(8,128)(2,1)S(1)} custom-call(bf16[384,512]{1,0:T(8,128)(2,1)S(1)} %get-tuple-element.35.refs_0_.refs_3_, bf16[384,512]{1,0:T(8,128)(2,1)S(1)} %get-tuple-element.36.refs_1_.refs_4_, f32[384,128]{1,0:T(8,128)S(1)} %get-tuple-element.37.refs_2_, bf16[2048,512]{1,0:T(8,128)(2,1)S(1)} %bitcast.46, ...), custom_call_target="tpu_custom_call" | custom-call | flops 805306368 | bytes 1048576 | tf_op jit(solution)/shard_map/input_grads/pallas_call | solution.py:202
  70.3 0.3 convert_add_fusion.1
  70.7 0.6 collective-permute-start.9
  71.3 4.5 %collective-permute-done.22 = bf16[2,2,104,512]{3,2,1,0:T(8,128)(2,1)S(1)} collective-permute-done((bf16[2,2,104,512]{3,2,1,0:T(8,128)(2,1)S(1)}, bf16[2,2,104,512]{3,2,1,0:T(8,128)(2,1)S(1)}, u32[]{:S(2)}, u32[]{:S(2)}) %collective-permute-start.22) | collective-permute-done | bytes 426016 | tf_op jit(solution)/shard_map/ppermute | solution.py:217
  75.9 1.4 %collective-permute-start.23 = (bf16[2,104,512]{2,1,0:T(8,128)(2,1)S(1)}, bf16[2,104,512]{2,1,0:T(8,128)(2,1)S(1)}, u32[]{:S(2)}, u32[]{:S(2)}) collective-permute-start(bf16[2,104,512]{2,1,0:T(8,128)(2,1)S(1)} %fusion.5), channel_id=1, source_target_pairs={{0,4},{1,3},{2,6},{3,1},{4,0},{5,7},{6,2},{7,5},{8,12},{9,11},{10,... | collective-permute-start | bytes 638984 | tf_op jit(solution)/shard_map/ppermute | solution.py:217
  77.4 5.0 %collective-permute-done.9 = bf16[2,2,104,512]{3,2,1,0:T(8,128)(2,1)S(1)} collective-permute-done((bf16[2,2,104,512]{3,2,1,0:T(8,128)(2,1)S(1)}, bf16[2,2,104,512]{3,2,1,0:T(8,128)(2,1)S(1)}, u32[]{:S(2)}, u32[]{:S(2)}) %collective-permute-start.9) | collective-permute-done | bytes 426016 | tf_op jit(solution)/shard_map/ppermute | solution.py:217
  82.4 0.1 slice_add_fusion.1
  82.6 1.4 %collective-permute-start.10 = (bf16[2,104,512]{2,1,0:T(8,128)(2,1)S(1)}, bf16[2,104,512]{2,1,0:T(8,128)(2,1)S(1)}, u32[]{:S(2)}, u32[]{:S(2)}) collective-permute-start(bf16[2,104,512]{2,1,0:T(8,128)(2,1)S(1)} %fusion.4), channel_id=1, source_target_pairs={{0,4},{1,3},{2,6},{3,1},{4,0},{5,7},{6,2},{7,5},{8,12},{9,11},{10,... | collective-permute-start | bytes 638984 | tf_op jit(solution)/shard_map/ppermute | solution.py:217
  84.1 4.4 %collective-permute-done.10 = bf16[2,104,512]{2,1,0:T(8,128)(2,1)S(1)} collective-permute-done((bf16[2,104,512]{2,1,0:T(8,128)(2,1)S(1)}, bf16[2,104,512]{2,1,0:T(8,128)(2,1)S(1)}, u32[]{:S(2)}, u32[]{:S(2)}) %collective-permute-start.10) | collective-permute-done | bytes 213024 | tf_op jit(solution)/shard_map/ppermute | solution.py:217
  88.7 3.1 %collective-permute-start.24 = (bf16[104,512]{1,0:T(8,128)(2,1)S(1)}, bf16[104,512]{1,0:T(8,128)(2,1)S(1)}, u32[]{:S(2)}, u32[]{:S(2)}) collective-permute-start(bf16[104,512]{1,0:T(8,128)(2,1)S(1)} %get-tuple-element.69), channel_id=1, source_target_pairs={{0,16},{1,17},{2,18},{3,19},{4,20},{5,21},{6,22},{7,23},{8,24},{9,... | collective-permute-start | bytes 319496 | tf_op jit(solution)/shard_map/ppermute | solution.py:214
  91.8 1.3 %collective-permute-start.25 = (bf16[104,512]{1,0:T(8,128)(2,1)S(1)}, bf16[104,512]{1,0:T(8,128)(2,1)S(1)}, u32[]{:S(2)}, u32[]{:S(2)}) collective-permute-start(bf16[104,512]{1,0:T(8,128)(2,1)S(1)} %get-tuple-element.68), channel_id=1, source_target_pairs={{0,24},{1,25},{2,26},{3,27},{4,28},{5,29},{6,30},{7,31},{8,16},{9,... | collective-permute-start | bytes 319496 | tf_op jit(solution)/shard_map/ppermute | solution.py:214
  93.0 6.0 %weight_grads.1 = (bf16[2048,512]{1,0:T(8,128)(2,1)}, bf16[2048,512]{1,0:T(8,128)(2,1)}, bf16[512,2048]{1,0:T(8,128)(2,1)}) custom-call(bf16[384,2048]{1,0:T(8,128)(2,1)S(1)} %get-tuple-element.50.refs_0_, bf16[384,2048]{1,0:T(8,128)(2,1)S(1)} %get-tuple-element.51.refs_1_, bf16[384,512]{1,0:T(8,128)(2,1)S(1)} %get-tuple-element.52.refs_2_, ...), custom_call_target="tpu_custom_call" | custom-call | flops 4831838208 | bytes 1048576 | tf_op jit(solution)/shard_map/weight_grads/pallas_call | solution.py:202
  99.1 1.2 %finish.1 = (bf16[128,512]{1,0:T(8,128)(2,1)}, f32[128,2]{1,0:T(8,128)S(1)}, f32[4,64]{1,0:T(4,128)}) custom-call(bf16[104,512]{1,0:T(8,128)(2,1)S(1)} %get-tuple-element.71.refs_0_, bf16[104,512]{1,0:T(8,128)(2,1)S(1)} %collective-permute-done.11.refs_1_, bf16[104,512]{1,0:T(8,128)(2,1)S(1)} %collective-permute-done.24.refs_2_, ...), custom_call_target="tpu_custom_call" | custom-call | tf_op jit(solution)/shard_map/finish/pallas_call | solution.py:494
  100.3 0.6 copy.13
  (61 shorter events, 1.0 us)
Async XLA Ops:
  0.6 1.0 %copy-start.5 = (bf16[128,2048]{1,0:T(8,128)(2,1)S(1)}, bf16[128,2048]{1,0:T(8,128)(2,1)}, u32[]{:S(2)}) copy-start(bf16[128,2048]{1,0:T(8,128)(2,1)} %tok_ref.1) | copy-start | bytes 1572868
  1.7 1.0 %copy-start.6 = (bf16[128,2048]{1,0:T(8,128)(2,1)S(1)}, bf16[128,2048]{1,0:T(8,128)(2,1)}, u32[]{:S(2)}) copy-start(bf16[128,2048]{1,0:T(8,128)(2,1)} %cot_ref.1) | copy-start | bytes 1572868
  2.7 0.7 copy-start.7
  3.4 0.7 copy-start.13
  5.1 24.4 %copy-start.9 = (f32[128,128]{1,0:T(8,128)}, f32[128,128]{1,0:T(8,128)S(1)}, u32[]{:S(2)}) copy-start(f32[128,128]{1,0:T(8,128)S(1)} %get-tuple-element.46.refs_7_) | copy-start | bytes 196612
  5.1 26.0 %copy-start.11 = (s32[128,128]{1,0:T(8,128)}, s32[128,128]{1,0:T(8,128)S(1)}, u32[]{:S(2)}) copy-start(s32[128,128]{1,0:T(8,128)S(1)} %get-tuple-element.47.refs_8_) | copy-start | bytes 196612
  5.1 8.8 %collective-permute-start = (bf16[104,1024]{1,0:T(8,128)(2,1)S(1)}, bf16[104,1024]{1,0:T(8,128)(2,1)S(1)}, u32[]{:S(2)}, u32[]{:S(2)}) collective-permute-start(bf16[104,1024]{1,0:T(8,128)(2,1)S(1)} %get-tuple-element.34), channel_id=1, source_target_pairs={{0,8},{1,9},{2,10},{3,11},{4,12},{5,13},{6,14},{7,15},{8,0},{9,1},... | collective-permute-start | bytes 638984 | tf_op jit(solution)/shard_map/ppermute | solution.py:214
  8.3 13.2 %collective-permute-start.13 = (bf16[104,1024]{1,0:T(8,128)(2,1)S(1)}, bf16[104,1024]{1,0:T(8,128)(2,1)S(1)}, u32[]{:S(2)}, u32[]{:S(2)}) collective-permute-start(bf16[104,1024]{1,0:T(8,128)(2,1)S(1)} %get-tuple-element.39), channel_id=1, source_target_pairs={{0,24},{1,25},{2,26},{3,27},{4,28},{5,29},{6,30},{7,31},{8,16},{9,... | collective-permute-start | bytes 638984 | tf_op jit(solution)/shard_map/ppermute | solution.py:214
  10.7 18.8 %collective-permute-start.12 = (bf16[104,1024]{1,0:T(8,128)(2,1)S(1)}, bf16[104,1024]{1,0:T(8,128)(2,1)S(1)}, u32[]{:S(2)}, u32[]{:S(2)}) collective-permute-start(bf16[104,1024]{1,0:T(8,128)(2,1)S(1)} %get-tuple-element.38), channel_id=1, source_target_pairs={{0,16},{1,17},{2,18},{3,19},{4,20},{5,21},{6,22},{7,23},{8,24},{9,... | collective-permute-start | bytes 638984 | tf_op jit(solution)/shard_map/ppermute | solution.py:214
  14.7 18.0 %collective-permute-start.1 = (bf16[2,104,1024]{2,1,0:T(8,128)(2,1)}, bf16[2,104,1024]{2,1,0:T(8,128)(2,1)}, u32[]{:S(2)}, u32[]{:S(2)}) collective-permute-start(bf16[2,104,1024]{2,1,0:T(8,128)(2,1)} %pad_maximum_fusion.refs_0_), channel_id=1, source_target_pairs={{0,4},{1,5},{2,6},{3,7},{4,0},{5,1},{6,2},{7,3},{8,12},{9,13},{10,... | collective-permute-start | bytes 1277960 | tf_op jit(solution)/shard_map/ppermute | solution.py:214
  16.2 16.5 %collective-permute-start.2 = (bf16[2,104,1024]{2,1,0:T(8,128)(2,1)}, bf16[2,104,1024]{2,1,0:T(8,128)(2,1)}, u32[]{:S(2)}, u32[]{:S(2)}) collective-permute-start(bf16[2,104,1024]{2,1,0:T(8,128)(2,1)} %pad_maximum_fusion.refs_0_), channel_id=1, source_target_pairs={{0,2},{1,3},{2,0},{3,1},{4,6},{5,7},{6,4},{7,5},{8,10},{9,11},{10,... | collective-permute-start | bytes 1277960 | tf_op jit(solution)/shard_map/ppermute | solution.py:214
  29.5 21.2 %copy-start = (bf16[1,2048,512]{2,1,0:T(8,128)(2,1)S(1)}, bf16[1,2048,512]{2,1,0:T(8,128)(2,1)}, u32[]{:S(2)}) copy-start(bf16[1,2048,512]{2,1,0:T(8,128)(2,1)} %param.11) | copy-start | bytes 6291460
  29.6 12.8 %collective-permute-start.14 = (bf16[2,104,1024]{2,1,0:T(8,128)(2,1)S(1)}, bf16[2,104,1024]{2,1,0:T(8,128)(2,1)S(1)}, u32[]{:S(2)}, u32[]{:S(2)}) collective-permute-start(bf16[2,104,1024]{2,1,0:T(8,128)(2,1)S(1)} %pad_maximum_fusion.1.refs_0_), channel_id=1, source_target_pairs={{0,4},{1,5},{2,6},{3,7},{4,0},{5,1},{6,2},{7,3},{8,12},{9,13},{10,... | collective-permute-start | bytes 1277960 | tf_op jit(solution)/shard_map/ppermute | solution.py:214
  31.1 11.2 %collective-permute-start.15 = (bf16[2,104,1024]{2,1,0:T(8,128)(2,1)S(1)}, bf16[2,104,1024]{2,1,0:T(8,128)(2,1)S(1)}, u32[]{:S(2)}, u32[]{:S(2)}) collective-permute-start(bf16[2,104,1024]{2,1,0:T(8,128)(2,1)S(1)} %pad_maximum_fusion.1.refs_0_), channel_id=1, source_target_pairs={{0,2},{1,3},{2,0},{3,1},{4,6},{5,7},{6,4},{7,5},{8,10},{9,11},{10,... | collective-permute-start | bytes 1277960 | tf_op jit(solution)/shard_map/ppermute | solution.py:214
  32.6 13.5 %collective-permute-start.4 = (bf16[2,104,1024]{2,1,0:T(8,128)(2,1)}, bf16[2,104,1024]{2,1,0:T(8,128)(2,1)S(1)}, u32[]{:S(2)}, u32[]{:S(2)}) collective-permute-start(bf16[2,104,1024]{2,1,0:T(8,128)(2,1)} %pad_maximum_fusion.refs_0_), channel_id=1, source_target_pairs={{0,1},{1,0},{2,3},{3,2},{4,5},{5,4},{6,7},{7,6},{8,9},{9,8},{10,11... | collective-permute-start | bytes 1277960 | tf_op jit(solution)/shard_map/ppermute | solution.py:214
  33.7 12.4 %collective-permute-start.3 = (bf16[2,104,1024]{2,1,0:T(8,128)(2,1)S(1)}, bf16[2,104,1024]{2,1,0:T(8,128)(2,1)S(1)}, u32[]{:S(2)}, u32[]{:S(2)}) collective-permute-start(bf16[2,104,1024]{2,1,0:T(8,128)(2,1)S(1)} %broadcast_select_fusion.1), channel_id=1, source_target_pairs={{0,2},{1,5},{2,0},{3,7},{4,6},{5,1},{6,4},{7,3},{8,10},{9,13},{10,... | collective-permute-start | bytes 1277960 | tf_op jit(solution)/shard_map/ppermute | solution.py:217
  34.3 12.3 %collective-permute-start.5 = (bf16[2,104,1024]{2,1,0:T(8,128)(2,1)}, bf16[2,104,1024]{2,1,0:T(8,128)(2,1)S(1)}, u32[]{:S(2)}, u32[]{:S(2)}) collective-permute-start(bf16[2,104,1024]{2,1,0:T(8,128)(2,1)} %collective-permute-done.1.refs_1_), channel_id=1, source_target_pairs={{0,1},{1,0},{2,3},{3,2},{4,5},{5,4},{6,7},{7,6},{8,9},{9,8},{10,11... | collective-permute-start | bytes 1277960 | tf_op jit(solution)/shard_map/ppermute | solution.py:214
  42.3 4.4 %collective-permute-start.6 = (bf16[2,104,1024]{2,1,0:T(8,128)(2,1)}, bf16[2,104,1024]{2,1,0:T(8,128)(2,1)S(1)}, u32[]{:S(2)}, u32[]{:S(2)}) collective-permute-start(bf16[2,104,1024]{2,1,0:T(8,128)(2,1)} %collective-permute-done.2.refs_2_), channel_id=1, source_target_pairs={{0,1},{1,0},{2,3},{3,2},{4,5},{5,4},{6,7},{7,6},{8,9},{9,8},{10,11... | collective-permute-start | bytes 1277960 | tf_op jit(solution)/shard_map/ppermute | solution.py:214
  42.4 8.3 %collective-permute-start.16 = (bf16[2,104,1024]{2,1,0:T(8,128)(2,1)S(1)}, bf16[2,104,1024]{2,1,0:T(8,128)(2,1)S(1)}, u32[]{:S(2)}, u32[]{:S(2)}) collective-permute-start(bf16[2,104,1024]{2,1,0:T(8,128)(2,1)S(1)} %broadcast_select_fusion), channel_id=1, source_target_pairs={{0,2},{1,5},{2,0},{3,7},{4,6},{5,1},{6,4},{7,3},{8,10},{9,13},{10,... | collective-permute-start | bytes 1277960 | tf_op jit(solution)/shard_map/ppermute | solution.py:217
  46.1 4.6 %collective-permute-start.7 = (bf16[2,104,1024]{2,1,0:T(8,128)(2,1)S(1)}, bf16[2,104,1024]{2,1,0:T(8,128)(2,1)S(1)}, u32[]{:S(2)}, u32[]{:S(2)}) collective-permute-start(bf16[2,104,1024]{2,1,0:T(8,128)(2,1)S(1)} %collective-permute-done.3.refs_3_), channel_id=1, source_target_pairs={{0,1},{1,0},{2,3},{3,2},{4,5},{5,4},{6,7},{7,6},{8,9},{9,8},{10,11... | collective-permute-start | bytes 1277960 | tf_op jit(solution)/shard_map/ppermute | solution.py:214
  46.1 13.2 %collective-permute-start.17 = (bf16[2,104,1024]{2,1,0:T(8,128)(2,1)S(1)}, bf16[2,104,1024]{2,1,0:T(8,128)(2,1)S(1)}, u32[]{:S(2)}, u32[]{:S(2)}) collective-permute-start(bf16[2,104,1024]{2,1,0:T(8,128)(2,1)S(1)} %pad_maximum_fusion.1.refs_0_), channel_id=1, source_target_pairs={{0,1},{1,0},{2,3},{3,2},{4,5},{5,4},{6,7},{7,6},{8,9},{9,8},{10,11... | collective-permute-start | bytes 1277960 | tf_op jit(solution)/shard_map/ppermute | solution.py:214
  46.6 12.7 %collective-permute-start.18 = (bf16[2,104,1024]{2,1,0:T(8,128)(2,1)S(1)}, bf16[2,104,1024]{2,1,0:T(8,128)(2,1)S(1)}, u32[]{:S(2)}, u32[]{:S(2)}) collective-permute-start(bf16[2,104,1024]{2,1,0:T(8,128)(2,1)S(1)} %collective-permute-done.14.refs_1_), channel_id=1, source_target_pairs={{0,1},{1,0},{2,3},{3,2},{4,5},{5,4},{6,7},{7,6},{8,9},{9,8},{10,11... | collective-permute-start | bytes 1277960 | tf_op jit(solution)/shard_map/ppermute | solution.py:214
  46.7 12.7 %collective-permute-start.19 = (bf16[2,104,1024]{2,1,0:T(8,128)(2,1)S(1)}, bf16[2,104,1024]{2,1,0:T(8,128)(2,1)S(1)}, u32[]{:S(2)}, u32[]{:S(2)}) collective-permute-start(bf16[2,104,1024]{2,1,0:T(8,128)(2,1)S(1)} %collective-permute-done.15.refs_2_), channel_id=1, source_target_pairs={{0,1},{1,0},{2,3},{3,2},{4,5},{5,4},{6,7},{7,6},{8,9},{9,8},{10,11... | collective-permute-start | bytes 1277960 | tf_op jit(solution)/shard_map/ppermute | solution.py:214
  50.7 8.7 %collective-permute-start.20 = (bf16[2,104,1024]{2,1,0:T(8,128)(2,1)S(1)}, bf16[2,104,1024]{2,1,0:T(8,128)(2,1)S(1)}, u32[]{:S(2)}, u32[]{:S(2)}) collective-permute-start(bf16[2,104,1024]{2,1,0:T(8,128)(2,1)S(1)} %collective-permute-done.16.refs_3_), channel_id=1, source_target_pairs={{0,1},{1,0},{2,3},{3,2},{4,5},{5,4},{6,7},{7,6},{8,9},{9,8},{10,11... | collective-permute-start | bytes 1277960 | tf_op jit(solution)/shard_map/ppermute | solution.py:214
  50.7 1.6 %copy-start.1 = (bf16[1,2048,512]{2,1,0:T(8,128)(2,1)S(1)}, bf16[1,2048,512]{2,1,0:T(8,128)(2,1)}, u32[]{:S(2)}) copy-start(bf16[1,2048,512]{2,1,0:T(8,128)(2,1)} %param.12) | copy-start | bytes 6291460
  52.3 1.6 %copy-start.3 = (bf16[1,512,2048]{2,1,0:T(8,128)(2,1)S(1)}, bf16[1,512,2048]{2,1,0:T(8,128)(2,1)}, u32[]{:S(2)}) copy-start(bf16[1,512,2048]{2,1,0:T(8,128)(2,1)} %param.13) | copy-start | bytes 6291460
  53.9 5.5 %copy-start.2 = (bf16[1,2048,512]{2,1,0:T(8,128)(2,1)S(1)}, bf16[1,2048,512]{2,1,0:T(8,128)(2,1)}, u32[]{:S(2)}) copy-start(bf16[1,2048,512]{2,1,0:T(8,128)(2,1)} %param.12) | copy-start | bytes 6291460
  53.9 5.5 %copy-start.4 = (bf16[1,512,2048]{2,1,0:T(8,128)(2,1)S(1)}, bf16[1,512,2048]{2,1,0:T(8,128)(2,1)}, u32[]{:S(2)}) copy-start(bf16[1,512,2048]{2,1,0:T(8,128)(2,1)} %param.13) | copy-start | bytes 6291460
  64.5 2.7 %collective-permute-start.21 = (bf16[4,2,104,512]{3,2,1,0:T(8,128)(2,1)S(1)}, bf16[4,2,104,512]{3,2,1,0:T(8,128)(2,1)S(1)}, u32[]{:S(2)}, u32[]{:S(2)}) collective-permute-start(bf16[4,2,104,512]{3,2,1,0:T(8,128)(2,1)S(1)} %input_grads.7), channel_id=1, source_target_pairs={{0,1},{1,0},{2,3},{3,2},{4,5},{5,4},{6,7},{7,6},{8,9},{9,8},{10,11... | collective-permute-start | bytes 2555912 | tf_op jit(solution)/shard_map/ppermute | solution.py:214
  66.1 4.2 %collective-permute-start.8 = (bf16[4,2,104,512]{3,2,1,0:T(8,128)(2,1)S(1)}, bf16[4,2,104,512]{3,2,1,0:T(8,128)(2,1)S(1)}, u32[]{:S(2)}, u32[]{:S(2)}) collective-permute-start(bf16[4,2,104,512]{3,2,1,0:T(8,128)(2,1)S(1)} %input_grads.5), channel_id=1, source_target_pairs={{0,1},{1,0},{2,3},{3,2},{4,5},{5,4},{6,7},{7,6},{8,9},{9,8},{10,11... | collective-permute-start | bytes 2555912 | tf_op jit(solution)/shard_map/ppermute | solution.py:214
  67.5 8.2 %collective-permute-start.22 = (bf16[2,2,104,512]{3,2,1,0:T(8,128)(2,1)S(1)}, bf16[2,2,104,512]{3,2,1,0:T(8,128)(2,1)S(1)}, u32[]{:S(2)}, u32[]{:S(2)}) collective-permute-start(bf16[2,2,104,512]{3,2,1,0:T(8,128)(2,1)S(1)} %slice.100), channel_id=1, source_target_pairs={{0,2},{1,5},{2,0},{3,7},{4,6},{5,1},{6,4},{7,3},{8,10},{9,13},{10,... | collective-permute-start | bytes 1277960 | tf_op jit(solution)/shard_map/ppermute | solution.py:217
  70.7 11.7 %collective-permute-start.9 = (bf16[2,2,104,512]{3,2,1,0:T(8,128)(2,1)S(1)}, bf16[2,2,104,512]{3,2,1,0:T(8,128)(2,1)S(1)}, u32[]{:S(2)}, u32[]{:S(2)}) collective-permute-start(bf16[2,2,104,512]{3,2,1,0:T(8,128)(2,1)S(1)} %slice.101), channel_id=1, source_target_pairs={{0,2},{1,5},{2,0},{3,7},{4,6},{5,1},{6,4},{7,3},{8,10},{9,13},{10,... | collective-permute-start | bytes 1277960 | tf_op jit(solution)/shard_map/ppermute | solution.py:217
  75.9 8.1 %collective-permute-start.23 = (bf16[2,104,512]{2,1,0:T(8,128)(2,1)S(1)}, bf16[2,104,512]{2,1,0:T(8,128)(2,1)S(1)}, u32[]{:S(2)}, u32[]{:S(2)}) collective-permute-start(bf16[2,104,512]{2,1,0:T(8,128)(2,1)S(1)} %fusion.5), channel_id=1, source_target_pairs={{0,4},{1,3},{2,6},{3,1},{4,0},{5,7},{6,2},{7,5},{8,12},{9,11},{10,... | collective-permute-start | bytes 638984 | tf_op jit(solution)/shard_map/ppermute | solution.py:217
  82.6 5.9 %collective-permute-start.10 = (bf16[2,104,512]{2,1,0:T(8,128)(2,1)S(1)}, bf16[2,104,512]{2,1,0:T(8,128)(2,1)S(1)}, u32[]{:S(2)}, u32[]{:S(2)}) collective-permute-start(bf16[2,104,512]{2,1,0:T(8,128)(2,1)S(1)} %fusion.4), channel_id=1, source_target_pairs={{0,4},{1,3},{2,6},{3,1},{4,0},{5,7},{6,2},{7,5},{8,12},{9,11},{10,... | collective-permute-start | bytes 638984 | tf_op jit(solution)/shard_map/ppermute | solution.py:217
  88.6 10.5 %collective-permute-start.11 = (bf16[104,512]{1,0:T(8,128)(2,1)S(1)}, bf16[104,512]{1,0:T(8,128)(2,1)S(1)}, u32[]{:S(2)}, u32[]{:S(2)}) collective-permute-start(bf16[104,512]{1,0:T(8,128)(2,1)S(1)} %get-tuple-element.70), channel_id=1, source_target_pairs={{0,8},{1,9},{2,10},{3,11},{4,12},{5,13},{6,14},{7,15},{8,0},{9,1},... | collective-permute-start | bytes 319496 | tf_op jit(solution)/shard_map/ppermute | solution.py:214
  88.7 10.4 %collective-permute-start.24 = (bf16[104,512]{1,0:T(8,128)(2,1)S(1)}, bf16[104,512]{1,0:T(8,128)(2,1)S(1)}, u32[]{:S(2)}, u32[]{:S(2)}) collective-permute-start(bf16[104,512]{1,0:T(8,128)(2,1)S(1)} %get-tuple-element.69), channel_id=1, source_target_pairs={{0,16},{1,17},{2,18},{3,19},{4,20},{5,21},{6,22},{7,23},{8,24},{9,... | collective-permute-start | bytes 319496 | tf_op jit(solution)/shard_map/ppermute | solution.py:214
  91.8 7.3 %collective-permute-start.25 = (bf16[104,512]{1,0:T(8,128)(2,1)S(1)}, bf16[104,512]{1,0:T(8,128)(2,1)S(1)}, u32[]{:S(2)}, u32[]{:S(2)}) collective-permute-start(bf16[104,512]{1,0:T(8,128)(2,1)S(1)} %get-tuple-element.68), channel_id=1, source_target_pairs={{0,24},{1,25},{2,26},{3,27},{4,28},{5,29},{6,30},{7,31},{8,16},{9,... | collective-permute-start | bytes 319496 | tf_op jit(solution)/shard_map/ppermute | solution.py:214
  93.0 6.0 %collective-permute-start.26 = (bf16[8,128]{1,0:T(8,128)(2,1)S(1)}, bf16[8,128]{1,0:T(8,128)(2,1)S(1)}, u32[]{:S(2)}, u32[]{:S(2)}) collective-permute-start(bf16[8,128]{1,0:T(8,128)(2,1)S(1)} %get-tuple-element.66), channel_id=1, source_target_pairs={{0,8},{1,9},{2,10},{3,11},{4,12},{5,13},{6,14},{7,15},{8,0},{9,1},... | collective-permute-start | bytes 6152 | tf_op jit(solution)/shard_map/ppermute | solution.py:214
  93.0 6.1 %copy-start.8 = (bf16[2048,4]{0,1:T(4,128)(2,1)S(1)}, bf16[2048,4]{0,1:T(4,128)(2,1)}, u32[]{:S(2)}) copy-start(bf16[2048,4]{0,1:T(4,128)(2,1)} %param.10) | copy-start | bytes 49156
  93.0 6.1 %copy-start.10 = (f32[128,128]{1,0:T(8,128)S(1)}, f32[128,128]{1,0:T(8,128)}, u32[]{:S(2)}) copy-start(f32[128,128]{1,0:T(8,128)} %copy-done.9) | copy-start | bytes 196612
  93.0 6.1 %copy-start.12 = (s32[128,128]{1,0:T(8,128)S(1)}, s32[128,128]{1,0:T(8,128)}, u32[]{:S(2)}) copy-start(s32[128,128]{1,0:T(8,128)} %copy-done.11) | copy-start | bytes 196612
